TPU v7x, 512 devices: a 8x2x16 block of a 8x8x16 slice. The times are simulated.
512 devices in a mesh: grp: 2 (over y), fs: 32 (over z, core), tp: 8 (over x).
Axes of the slice: x: 8, y: 2, z: 16, core: 2. Of those that a mesh axis runs over, the one named last changes fastest.
The devices are a block of a 8x8x16 slice.
Arguments:
- tokens: bfloat16 [49152, 2048], P(('grp', 'fs')), parts along dimension 0, may hold values from -6 to 6
- pre_gain: float32 [2048], replicated, may hold values from 0.1 to 1.9
- up_weight: bfloat16 [2048, 8192], P('fs', 'tp'), may hold values from -0.125 to 0.125
- down_weight: bfloat16 [8192, 2048], P(('tp', 'fs')), as said below
- post_gain: float32 [2048], P('tp'), may hold values from 0.1 to 1.9
Outputs:
- mixed: bfloat16 [49152, 2048], P(('grp', 'fs'), 'tp'), parts along dimension 0
There are 2 independent parts, one for each index of `grp`. A program takes and returns all parts, laid end to end along the dimension named above; an argument that names none is the same for every part. Nothing has to cross between parts.
Inputs may be any that keep to these rules, and one draw needn't show every extreme that they name: `down_weight`: a matrix whose columns fall into 8 consecutive blocks of different magnitudes.
All inputs are finite; a program needn't handle non-finite values.
Results may differ from a plain program's by a relative error of at most 0.014.
Values may be sent and summed in bfloat16 or wider, within the bound.
No kernel may reach another device: no remote copies, remote signals or barrier semaphores. Data moves between devices by JAX's collectives and lax.ppermute only.
A program may use at most 64 MiB of HBM per device.

v0:
```python
import jax
import jax.numpy as jnp
from jax import lax
from jax.sharding import PartitionSpec as P


def from_everyone(value, axis):
    copies = jnp.broadcast_to(value, (lax.axis_size(axis), *value.shape))
    return lax.all_to_all(copies, axis, split_axis=0, concat_axis=0, tiled=True)


def of_everyone(value, axis):
    everything = from_everyone(value, axis)
    return jnp.sum(everything, axis=0)


def shards(tokens, pre_gain, up_weight, down_weight, post_gain):
    eps = 1e-06
    values = tokens.astype(jnp.float32)
    normed = (
        values * lax.rsqrt(jnp.mean(values * values, axis=1, keepdims=True) + eps) * pre_gain
    ).astype(jnp.bfloat16)
    full_up = lax.all_gather(up_weight, "fs", axis=0, tiled=True)
    up = jnp.dot(normed, full_up, preferred_element_type=jnp.float32)
    hidden = jnp.square(jnp.maximum(up, 0.0)).astype(jnp.bfloat16)
    full_down = lax.all_gather(down_weight, "fs", axis=0, tiled=True)
    partial_terms = jnp.dot(hidden, full_down, preferred_element_type=jnp.float32)
    own_width = post_gain.shape[0]
    full_width = lax.axis_size("tp") * own_width
    mixed = lax.psum_scatter(
        partial_terms.astype(jnp.bfloat16), "tp", scatter_dimension=1, tiled=True
    ).astype(jnp.float32)
    squares = of_everyone(jnp.sum(mixed * mixed, axis=1), "tp")
    factor = lax.rsqrt(squares / full_width + eps)
    return (mixed * factor[:, None] * post_gain).astype(jnp.bfloat16)


def solution(mesh):
    in_specs = (P(("grp", "fs"), None), P(), P("fs", "tp"), P(("tp", "fs"), None), P("tp"))
    out_specs = P(("grp", "fs"), "tp")
    return jax.shard_map(shards, mesh=mesh, in_specs=in_specs, out_specs=out_specs, check_vma=False)
```

profile of v0, /device:TPU:80, one launch (start us, length us, event | category | flops | bytes accessed | tf_op | source)
XLA Modules:
  0.0 276.5 jit_solution(11788254822530695239)
XLA Ops:
  6.5 0.0 all-gather.3.cloned.1.call-start
  6.6 0.7 all-gather.3.cloned.1.call-update
  7.3 0.1 all-gather.5.cloned.1.call-start
  7.4 0.7 all-gather.5.cloned.1.call-update
  8.1 0.1 reduce-scatter.2.cloned.1.call-start
  8.2 2.6 fusion
  10.8 0.0 copy-start
  10.8 106.7 %all-gather.3.cloned.1.call-done = bf16[2048,1024]{1,0:T(8,128)(2,1)} async-done(((bf16[64,1024]{1,0:T(8,128)(2,1)}), bf16[2048,1024]{1,0:T(8,128)(2,1)}) %all-gather.3.cloned.1.call-update) | async-done | bytes 4194320 | tf_op jit(solution)/shard_map/all_gather | solution.py:23
  117.5 74.3 %all-gather.5.cloned.1.call-done = bf16[1024,2048]{1,0:T(8,128)(2,1)} async-done(((bf16[32,2048]{1,0:T(8,128)(2,1)}), bf16[1024,2048]{1,0:T(8,128)(2,1)}) %all-gather.5.cloned.1.call-update) | async-done | bytes 4194320 | tf_op jit(solution)/shard_map/all_gather | solution.py:26
  191.9 12.1 %convolution_convert_fusion = bf16[768,2048]{1,0:T(8,128)(2,1)} fusion(bf16[1024,2048]{1,0:T(8,128)(2,1)} %all-gather.5.cloned.1.call-done, bf16[2048,1024]{1,0:T(8,128)(2,1)} %all-gather.3.cloned.1.call-done, bf16[768,2048]{1,0:T(8,128)(2,1)} %param.5, f32[2048]{0:T(1024)} %param.6, f32[768]{0:T(1024)S(1)} %add_rsqrt_fusion.1), kind=kOutput, calls=%fused_computation.5 | convolution fusion | flops 6452674560 | bytes 14691328 | tf_op jit(solution)/shard_map/dot_general | solution.py:27
  204.0 0.1 reduce-scatter.2.cloned.1.call-update
  204.1 49.9 %reduce-scatter.2.cloned.1.call-done = bf16[768,256]{1,0:T(8,128)(2,1)} async-done(((bf16[768,2048]{1,0:T(8,128)(2,1)}), bf16[768,256]{1,0:T(8,128)(2,1)}) %reduce-scatter.2.cloned.1.call-update) | async-done | bytes 393232 | tf_op jit(solution)/shard_map/reduce_scatter | solution.py:30
  253.9 1.2 fusion.9
  255.2 12.8 %all_to_all.6 = f32[8,1,768]{2,1,0:T(1,128)S(1)} all-to-all(f32[8,1,768]{2,1,0:T(1,128)S(1)} %broadcast_in_dim.2), channel_id=1, replica_groups=mesh['grp'=2,'fs'=32,'tp'=8] {'tp'}, dimensions={0} | all-to-all | bytes 49152 | tf_op jit(solution)/shard_map/all_to_all | solution.py:9
  268.0 0.0 copy-done
  268.0 1.9 fusion.11
  (4 shorter events, 0.1 us)
Async XLA Ops:
  6.5 111.0 %all-gather.3.cloned.1.call-start = ((), (), s32[]{:S(2)}) async-start(), calls=%async_computation.2 | async-start | bytes 4325376 | tf_op jit(solution)/shard_map/all_gather | solution.py:23
  7.3 184.6 %all-gather.5.cloned.1.call-start = ((), (), s32[]{:S(2)}) async-start(), calls=%async_computation.3 | async-start | bytes 4325376 | tf_op jit(solution)/shard_map/all_gather | solution.py:26
  8.1 245.8 %reduce-scatter.2.cloned.1.call-start = ((), (), s32[]{:S(2)}) async-start(), calls=%async_computation.4 | async-start | bytes 3538944 | tf_op jit(solution)/shard_map/reduce_scatter | solution.py:30
  10.8 257.3 %copy-start = (f32[256]{0:T(256)S(1)}, f32[256]{0:T(256)}, u32[]{:S(2)}) copy-start(f32[256]{0:T(256)} %param.9) | copy-start | bytes 3076
Sparse Core Ops, SparseCore 0:
  9.5 107.9 all-gather.2
  119.7 72.1 all-gather.4
  204.2 49.7 reduce-scatter.1
where the time goes:
time: 277 us; the launch traced here: 276 us
  waiting for transfers between devices  233 us (84%)
  between operations  13.2 us (5%)
  blocking collectives  12.8 us (5%)
  matrix products  12.1 us (4%)
  other arithmetic  5.7 us (2%)
    all_gather x1, waiting for transfers between devices, shards(): full_up = lax.all_gather(up_weight, 'fs', axis=0, tiled=True)  107 us
    all_gather x1, waiting for transfers between devices, shards(): full_down = lax.all_gather(down_weight, 'fs', axis=0, tiled=True)  74.3 us
    reduce_scatter x1, waiting for transfers between devices, shards(): lax.psum_scatter(partial_terms.astype(jnp.bfloat16), 'tp', scatter_dimens...  49.9 us
    all_to_all x1, blocking collectives, from_everyone(): return lax.all_to_all(copies, axis, split_axis=0, concat_axis=0, tiled=True)  12.8 us
    dot_general x1, matrix products, shards(): jnp.dot(hidden, full_down, preferred_element_type=jnp.float32)  12.1 us
  transfers between devices with their start and end apart: 3, of which 3 were waited for; matrix products, arithmetic and copies ran while one was open for 1% of the time, Pallas kernels for 0%

commit v1 on v0

v1 whole, which is shorter than its diff:
```python
import functools

import jax
import jax.numpy as jnp
from jax import lax
from jax.experimental import pallas as pl
from jax.experimental.pallas import tpu as pltpu
from jax.sharding import PartitionSpec as P


def from_everyone(value, axis):
    copies = jnp.broadcast_to(value, (lax.axis_size(axis), *value.shape))
    return lax.all_to_all(copies, axis, split_axis=0, concat_axis=0, tiled=True)


def of_everyone(value, axis):
    everything = from_everyone(value, axis)
    return jnp.sum(everything, axis=0)


def norm_kernel(x_ref, gain_ref, out_ref):
    x = x_ref[...].astype(jnp.float32)
    factor = lax.rsqrt(jnp.mean(x * x, axis=1, keepdims=True) + 1e-6)
    out_ref[...] = (x * factor * gain_ref[...]).astype(jnp.bfloat16)


def norm(tokens, gain, rows):
    count, width = tokens.shape
    return pl.pallas_call(
        norm_kernel,
        grid=(count // rows,),
        in_specs=[
            pl.BlockSpec((rows, width), lambda i: (i, 0)),
            pl.BlockSpec((1, width), lambda i: (0, 0)),
        ],
        out_specs=pl.BlockSpec((rows, width), lambda i: (i, 0)),
        out_shape=jax.ShapeDtypeStruct((count, width), jnp.bfloat16),
        name="pre_norm",
    )(tokens, gain.reshape(1, width))


def layer_kernel(packed, x_ref, out_ref, up_v, down_v, hidden_v, up_sem, down_sem, *, shards, up_rows, down_rows):
    step = pl.program_id(0)
    width = up_v.shape[1]
    cols = out_ref.shape[1]
    parts = down_v.shape[1] // width
    rows = up_rows + parts * down_rows

    def up_copy(s):
        return pltpu.make_async_copy(
            packed.at[pl.ds(s * rows, up_rows)], up_v.at[pl.ds(s * up_rows, up_rows)], up_sem.at[s]
        )

    def down_copy(s, p):
        return pltpu.make_async_copy(
            packed.at[pl.ds(s * rows + up_rows + p * down_rows, down_rows)],
            down_v.at[pl.ds(s * down_rows, down_rows), pl.ds(p * width, width)],
            down_sem.at[p * shards + s],
        )

    @pl.when(step == 0)
    def _():
        def start_up(s, c):
            up_copy(s).start()
            return c

        lax.fori_loop(0, shards, start_up, 0)
        for p in range(parts):
            def start_down(s, c, p=p):
                down_copy(s, p).start()
                return c

            lax.fori_loop(0, shards, start_down, 0)

        def wait_up(s, c):
            up_copy(s).wait()
            return c

        lax.fori_loop(0, shards, wait_up, 0)
        piece = 512
        for n in range(width // piece):
            span = slice(n * piece, (n + 1) * piece)
            up = jnp.dot(x_ref[...], up_v[:, span], preferred_element_type=jnp.float32)
            hidden_v[:, span] = jnp.square(jnp.maximum(up, 0.0)).astype(jnp.bfloat16)

        for p in range(parts):
            def wait_down(s, c, p=p):
                down_copy(s, p).wait()
                return c

            lax.fori_loop(0, shards, wait_down, 0)

    start = pl.multiple_of(step * cols, cols)
    out_ref[...] = jnp.dot(
        hidden_v[...], down_v[:, pl.ds(start, cols)], preferred_element_type=jnp.float32
    ).astype(jnp.bfloat16)


def layer(packed, normed, shards, up_rows, down_rows):
    count, width = normed.shape
    hidden = packed.shape[1]
    cols = 512
    return pl.pallas_call(
        functools.partial(layer_kernel, shards=shards, up_rows=up_rows, down_rows=down_rows),
        grid=(width // cols,),
        in_specs=[
            pl.BlockSpec(memory_space=pl.ANY),
            pl.BlockSpec((count, width), lambda j: (0, 0)),
        ],
        out_specs=pl.BlockSpec((count, cols), lambda j: (0, j)),
        out_shape=jax.ShapeDtypeStruct((count, width), jnp.bfloat16),
        scratch_shapes=[
            pltpu.VMEM((width, hidden), jnp.bfloat16),
            pltpu.VMEM((hidden, width), jnp.bfloat16),
            pltpu.VMEM((count, hidden), jnp.bfloat16),
            pltpu.SemaphoreType.DMA((shards,)),
            pltpu.SemaphoreType.DMA((shards * (width // hidden),)),
        ],
        compiler_params=pltpu.CompilerParams(vmem_limit_bytes=40 * 1024 * 1024),
        name="layer",
    )(packed, normed)


def shards(tokens, pre_gain, up_weight, down_weight, post_gain):
    eps = 1e-06
    fs = lax.axis_size("fs")
    hidden = up_weight.shape[1]
    width = down_weight.shape[1]
    pieces = [up_weight] + [down_weight[:, p * hidden:(p + 1) * hidden] for p in range(width // hidden)]
    packed = lax.all_gather(jnp.concatenate(pieces, axis=0), "fs", axis=0, tiled=True)
    normed = norm(tokens, pre_gain, 256)
    partial_terms = layer(packed, normed, fs, up_weight.shape[0], down_weight.shape[0])
    own_width = post_gain.shape[0]
    full_width = lax.axis_size("tp") * own_width
    mixed = lax.psum_scatter(partial_terms, "tp", scatter_dimension=1, tiled=True).astype(jnp.float32)
    squares = of_everyone(jnp.sum(mixed * mixed, axis=1), "tp")
    factor = lax.rsqrt(squares / full_width + eps)
    return (mixed * factor[:, None] * post_gain).astype(jnp.bfloat16)


def solution(mesh):
    in_specs = (P(("grp", "fs"), None), P(), P("fs", "tp"), P(("tp", "fs"), None), P("tp"))
    out_specs = P(("grp", "fs"), "tp")
    return jax.shard_map(shards, mesh=mesh, in_specs=in_specs, out_specs=out_specs, check_vma=False)
```

time: 277 us -> 210 us (0.76)
  waiting for transfers between devices: 233 us -> 158 us
  Pallas kernels: 0 us -> 16.9 us
  matrix products: 12.1 us -> 0 us
  local copies, waits for them, and re-layouts: 0.02 us -> 2.79 us
    all_gather x2 -> x1, waiting for transfers between devices: 181 us -> 109 us  [shards(): lax.all_gather(jnp.concatenate(pieces, axis=0), 'fs', axis=0, tiled=True)]
    pallas_call x0 -> x2, Pallas kernels: none -> 16.9 us  [the longest x1 11.9 us: layer(): pl.pallas_call(functools.partial(layer_kernel, shards=shards, up_rows=up_...]
    dot_general x1 -> x0, matrix products: 12.1 us -> none  [shards(): jnp.dot(hidden, full_down, preferred_element_type=jnp.float32)]
  transfers between devices with their start and end apart: 3 -> 2, of which waited for: 3 -> 2; matrix products, arithmetic and copies ran while one was open for 1% -> 0% of each run, Pallas kernels for 0% -> 2%
where the time goes in v1:
time: 210 us; the launch traced here: 209 us
  waiting for transfers between devices  158 us (75%)
  Pallas kernels  16.9 us (8%)
  between operations  13.5 us (6%)
  blocking collectives  12.8 us (6%)
  other arithmetic  4.75 us (2%)
  local copies, waits for them, and re-layouts  2.79 us (1%)
    all_gather x1, waiting for transfers between devices, shards(): lax.all_gather(jnp.concatenate(pieces, axis=0), 'fs', axis=0, tiled=True)  109 us
    reduce_scatter x1, waiting for transfers between devices, shards(): lax.psum_scatter(partial_terms, 'tp', scatter_dimension=1, tiled=True)  49.3 us
    all_to_all x1, blocking collectives, from_everyone(): return lax.all_to_all(copies, axis, split_axis=0, concat_axis=0, tiled=True)  12.8 us
    pallas_call x1, Pallas kernels, layer(): pl.pallas_call(functools.partial(layer_kernel, shards=shards, up_rows=up_...  11.9 us
    pallas_call x1, Pallas kernels, norm(): pl.pallas_call(norm_kernel, grid=(count // rows,), in_specs=[pl.BlockSpec...  5.02 us
  transfers between devices with their start and end apart: 2, of which 2 were waited for; matrix products, arithmetic and copies ran while one was open for 0% of the time, Pallas kernels for 2%

profile of v1, /device:TPU:80, one launch (start us, length us, event | category | flops | bytes accessed | tf_op | source)
XLA Modules:
  0.0 208.9 jit_solution(10091852184665538773)
XLA Ops:
  6.5 0.0 all-gather.2.cloned.1.call-start
  6.6 0.9 fusion.3
  7.4 1.6 pad_maximum_fusion
  9.1 0.1 all-gather.2.cloned.1.call-update
  9.1 0.1 reduce-scatter.2.cloned.1.call-start
  9.2 5.0 %pre_norm.1.x_ref = bf16[768,2048]{1,0:T(8,128)(2,1)} custom-call(bf16[768,2048]{1,0:T(8,128)(2,1)} %x_ref.1, f32[1,2048]{1,0:T(1,128)} %bitcast.1), custom_call_target="tpu_custom_call" | custom-call | tf_op jit(solution)/shard_map/pre_norm/pallas_call | solution.py:29
  14.2 108.7 %all-gather.2.cloned.1.call-done.packed = bf16[4096,1024]{1,0:T(8,128)(2,1)} async-done(((bf16[128,1024]{1,0:T(8,128)(2,1)}), bf16[4096,1024]{1,0:T(8,128)(2,1)}) %all-gather.2.cloned.1.call-update) | async-done | bytes 8388624 | tf_op jit(solution)/shard_map/all_gather | solution.py:130
  122.9 0.0 copy-start
  122.9 1.9 copy-done
  124.8 11.9 %layer.1 = bf16[768,2048]{1,0:T(8,128)(2,1)} custom-call(bf16[4096,1024]{1,0:T(8,128)(2,1)} %all-gather.2.cloned.1.call-done.packed, bf16[768,2048]{1,0:T(8,128)(2,1)S(1)} %copy-done), custom_call_target="tpu_custom_call" | custom-call | tf_op jit(solution)/shard_map/layer/pallas_call | solution.py:103
  136.6 0.0 copy-start.1
  136.6 0.1 reduce-scatter.2.cloned.1.call-update
  136.7 49.3 %reduce-scatter.2.cloned.1.call-done = bf16[768,256]{1,0:T(8,128)(2,1)} async-done(((bf16[768,2048]{1,0:T(8,128)(2,1)}), bf16[768,256]{1,0:T(8,128)(2,1)}) %reduce-scatter.2.cloned.1.call-update) | async-done | bytes 393232 | tf_op jit(solution)/shard_map/reduce_scatter | solution.py:135
  186.0 1.2 fusion
  187.2 12.8 %all_to_all.6 = f32[8,1,768]{2,1,0:T(1,128)S(1)} all-to-all(f32[8,1,768]{2,1,0:T(1,128)S(1)} %broadcast_in_dim.2), channel_id=1, replica_groups=mesh['grp'=2,'fs'=32,'tp'=8] {'tp'}, dimensions={0} | all-to-all | bytes 49152 | tf_op jit(solution)/shard_map/all_to_all | solution.py:13
  200.1 0.0 copy-done.1
  200.1 1.9 fusion.2
  (3 shorter events, 0.1 us)
Async XLA Ops:
  6.5 116.3 %all-gather.2.cloned.1.call-start = ((), (), s32[]{:S(2)}) async-start(), calls=%async_computation.2 | async-start | bytes 8650752 | tf_op jit(solution)/shard_map/all_gather | solution.py:130
  9.1 176.9 %reduce-scatter.2.cloned.1.call-start = ((), (), s32[]{:S(2)}) async-start(), calls=%async_computation.3 | async-start | bytes 3538944 | tf_op jit(solution)/shard_map/reduce_scatter | solution.py:135
  122.9 1.9 copy-start
  136.6 63.5 %copy-start.1 = (f32[256]{0:T(256)S(1)}, f32[256]{0:T(256)}, u32[]{:S(2)}) copy-start(f32[256]{0:T(256)} %param.9) | copy-start | bytes 3076
Sparse Core Ops, SparseCore 0:
  9.5 113.3 all-gather.1
  136.8 49.1 reduce-scatter.1

commit v2 on v0

v2 whole, which is shorter than its diff:
```python
import functools

import jax
import jax.numpy as jnp
from jax import lax
from jax.experimental import pallas as pl
from jax.experimental.pallas import tpu as pltpu
from jax.sharding import PartitionSpec as P

LANES = 1024
TOP = 2.0 ** 15
UP_FACTORS = 3
DOWN_FACTORS = 5


def from_everyone(value, axis):
    copies = jnp.broadcast_to(value, (lax.axis_size(axis), *value.shape))
    return lax.all_to_all(copies, axis, split_axis=0, concat_axis=0, tiled=True)


def of_everyone(value, axis):
    everything = from_everyone(value, axis)
    return jnp.sum(everything, axis=0)


def power_factors(top, count):
    factors = []
    for _ in range(count):
        factor = jnp.ones_like(top)
        for power in (8, 4, 2):
            factor = jnp.where(top * factor * 2.0**power <= TOP, factor * 2.0**power, factor)
        for power in (8, 4, 2):
            factor = jnp.where(top * factor > TOP * 2.0 ** (power - 2), factor * 2.0**-power, factor)
        top = top * factor
        factors.append(factor)
    return factors


def largest(value):
    return jnp.max(jnp.max(jnp.abs(value), axis=0, keepdims=True), axis=1, keepdims=True)


def pack_kernel(order_ref, up_ref, down_ref, out_ref, *, own):
    up_rows = up_ref.shape[0]
    down_rows = down_ref.shape[0]
    up = up_ref[...].astype(jnp.float32)
    up_factors = power_factors(jnp.broadcast_to(largest(up), (1, LANES)), UP_FACTORS)
    for factor in up_factors:
        up = up * factor
    out_ref[0:up_rows, :] = up.astype(jnp.bfloat16)
    top = largest(down_ref[...].astype(jnp.float32))
    down_factors = power_factors(jnp.broadcast_to(top, (1, LANES)), DOWN_FACTORS)
    for j in range(down_ref.shape[1] // own):
        start = pl.multiple_of(order_ref[j] * own, own)
        piece = down_ref[:, pl.ds(start, own)].astype(jnp.float32)
        for factor in down_factors:
            piece = piece * factor[:, :own]
        row = up_rows + down_rows * (j * own // LANES)
        column = j * own % LANES
        out_ref[row:row + down_rows, column:column + own] = piece.astype(jnp.bfloat16)
    row = up_rows + down_rows * (down_ref.shape[1] // LANES)
    inverses = [1.0 / factor for factor in up_factors + down_factors]
    out_ref[row:, :] = jnp.concatenate(inverses, axis=0).astype(jnp.bfloat16)


def pack(order, up_weight, down_weight, own):
    rows = up_weight.shape[0] + down_weight.shape[0] * (down_weight.shape[1] // LANES)
    return pl.pallas_call(
        functools.partial(pack_kernel, own=own),
        in_specs=[
            pl.BlockSpec(memory_space=pltpu.SMEM),
            pl.BlockSpec(memory_space=pltpu.VMEM),
            pl.BlockSpec(memory_space=pltpu.VMEM),
        ],
        out_shape=jax.ShapeDtypeStruct((rows + UP_FACTORS + DOWN_FACTORS, LANES), jnp.bfloat16),
        name="pack",
    )(order, up_weight, down_weight)


def first_kernel(x_ref, gain_ref, up_ref, inverse_ref, down_ref, hidden_ref, part_ref, up_scale, down_scale):
    shards = inverse_ref.shape[0]

    @pl.when(pl.program_id(0) == 0)
    def _():
        for scale, first, count in ((up_scale, 0, UP_FACTORS), (down_scale, UP_FACTORS, DOWN_FACTORS)):
            width = scale.shape[1]
            per = width // shards
            for p in range(width // LANES):
                owner = (lax.broadcasted_iota(jnp.int32, (1, LANES), 1) + p * LANES) // per
                total = jnp.zeros((1, LANES), jnp.float32)
                for s in range(p * LANES // per, ((p + 1) * LANES - 1) // per + 1):
                    rows = inverse_ref[s].astype(jnp.float32)
                    value = rows[first:first + 1]
                    for t in range(1, count):
                        value = value * rows[first + t:first + t + 1]
                    value = jnp.concatenate([value] * (LANES // value.shape[1]), axis=1)
                    total = jnp.where(owner == s, value, total)
                scale[:, p * LANES:(p + 1) * LANES] = total

    x = x_ref[...].astype(jnp.float32)
    factor = lax.rsqrt(jnp.mean(x * x, axis=1, keepdims=True) + 1e-6)
    normed = (x * factor * gain_ref[...]).astype(jnp.bfloat16) * up_scale[...].astype(jnp.bfloat16)
    up = jnp.dot(normed, up_ref[...], preferred_element_type=jnp.float32)
    hidden = (jnp.square(jnp.maximum(up, 0.0)) * down_scale[...]).astype(jnp.bfloat16)
    hidden_ref[...] = hidden
    part_ref[...] = jnp.dot(hidden, down_ref[...], preferred_element_type=jnp.float32).astype(jnp.bfloat16)


def first(tokens, gain, up, inverses, down, start, rows):
    width = tokens.shape[1]
    hidden = up.shape[1]
    own = down.shape[1]
    whole = lambda *shape: pl.BlockSpec(shape, lambda i: (0,) * len(shape))
    return pl.pallas_call(
        first_kernel,
        grid=(1,),
        in_specs=[
            pl.BlockSpec((rows, width), lambda i: (start, 0)),
            whole(1, width),
            whole(*up.shape),
            whole(*inverses.shape),
            whole(*down.shape),
        ],
        out_specs=[whole(rows, hidden), whole(rows, own)],
        out_shape=[
            jax.ShapeDtypeStruct((rows, hidden), jnp.bfloat16),
            jax.ShapeDtypeStruct((rows, own), jnp.bfloat16),
        ],
        scratch_shapes=[pltpu.VMEM((1, width), jnp.float32), pltpu.VMEM((1, hidden), jnp.float32)],
        compiler_params=pltpu.CompilerParams(vmem_limit_bytes=24 * 1024 * 1024),
        name="first",
    )(tokens, gain.reshape(1, width), up, inverses, down)


def rest_kernel(top_ref, bottom_ref, down_ref, out_ref):
    half = top_ref.shape[0]
    own = out_ref.shape[2]
    for j in range(out_ref.shape[0]):
        down = down_ref[:, j * own:(j + 1) * own]
        for at, hidden_ref in ((0, top_ref), (half, bottom_ref)):
            part = jnp.dot(hidden_ref[...], down, preferred_element_type=jnp.float32)
            out_ref[j, at:at + half, :] = part.astype(jnp.bfloat16)


def rest(top, bottom, down, own):
    return pl.pallas_call(
        rest_kernel,
        out_shape=jax.ShapeDtypeStruct((down.shape[1] // own, 2 * top.shape[0], own), jnp.bfloat16),
        compiler_params=pltpu.CompilerParams(vmem_limit_bytes=16 * 1024 * 1024),
        name="rest",
    )(top, bottom, down)


def add(a, b):
    return (a.astype(jnp.float32) + b.astype(jnp.float32)).astype(jnp.bfloat16)


def shards(tokens, pre_gain, up_weight, down_weight, post_gain):
    eps = 1e-06
    fs = lax.axis_size("fs")
    tp = lax.axis_size("tp")
    me = lax.axis_index("tp")
    up_rows, down_rows = up_weight.shape[0], down_weight.shape[0]
    own = post_gain.shape[0]
    half = tokens.shape[0] // 2
    offsets = [tp // 2]
    for distance in range(tp // 2 - 1, 0, -1):
        offsets += [distance, tp - distance]
    offsets.append(0)
    order = (me + jnp.array(offsets, jnp.int32)) % tp
    packed = pack(order, up_weight, down_weight, own)
    rows = packed.shape[0]
    scales = UP_FACTORS + DOWN_FACTORS
    everything = lax.all_gather(packed.astype(jnp.float16), "fs", axis=0, tiled=False)

    def down(source, start, stop):
        pieces = []
        while start < stop:
            column = start * own % LANES
            width = min((stop - start) * own, LANES - column)
            row = up_rows + down_rows * (start * own // LANES)
            piece = source[:, row:row + down_rows, column:column + width].astype(jnp.bfloat16)
            pieces.append(piece.reshape(fs * down_rows, width))
            start += width // own
        return pieces

    up = everything[:, :up_rows].astype(jnp.bfloat16).reshape(fs * up_rows, LANES)
    inverses = everything[:, rows - scales:, :128].astype(jnp.bfloat16)
    far_down, = down(everything, 0, 1)
    top, top_part = first(tokens, pre_gain, up, inverses, far_down, 0, half)
    bottom, bottom_part = first(tokens, pre_gain, up, inverses, far_down, 1, half)

    right = [(i, (i + 1) % tp) for i in range(tp)]
    left = [(i, (i - 1) % tp) for i in range(tp)]
    from_left = lax.ppermute(top_part, "tp", right)
    from_right = lax.ppermute(bottom_part, "tp", left)
    held, bottom = lax.optimization_barrier((everything, bottom))
    parts = []
    for piece in down(held, 1, 3):
        got = rest(top, bottom, piece, own)
        parts += [got[j] for j in range(got.shape[0])]
    for step in range(tp // 2 - 1):
        to_right, to_left = parts[2 * step], parts[2 * step + 1]
        if step == 0:
            to_right = jnp.concatenate([add(from_left, to_right[:half]), to_right[half:]], axis=0)
            to_left = jnp.concatenate([to_left[:half], add(from_right, to_left[half:])], axis=0)
        else:
            to_right = add(from_left, to_right)
            to_left = add(from_right, to_left)
        from_left = lax.ppermute(to_right, "tp", right)
        from_right = lax.ppermute(to_left, "tp", left)
        if step == 0:
            held, to_right = lax.optimization_barrier((held, to_right))
            for piece in down(held, 3, tp):
                got = rest(top, bottom, piece, own)
                parts += [got[j] for j in range(got.shape[0])]
    mixed = parts[-1].astype(jnp.float32) + from_left.astype(jnp.float32) + from_right.astype(jnp.float32)
    squares = of_everyone(jnp.sum(mixed * mixed, axis=1), "tp")
    factor = lax.rsqrt(squares / (tp * own) + eps)
    return (mixed * factor[:, None] * post_gain).astype(jnp.bfloat16)


def solution(mesh):
    in_specs = (P(("grp", "fs"), None), P(), P("fs", "tp"), P(("tp", "fs"), None), P("tp"))
    out_specs = P(("grp", "fs"), "tp")
    return jax.shard_map(shards, mesh=mesh, in_specs=in_specs, out_specs=out_specs, check_vma=False)
```

time: 277 us -> 184 us (0.66)
  waiting for transfers between devices: 233 us -> 22.2 us
  blocking collectives: 12.8 us -> 115 us
  starting transfers between devices: 0.12 us -> 29.5 us
  between operations: 13.2 us -> 0.25 us
  matrix products: 12.1 us -> 0 us
  Pallas kernels: 0 us -> 10.5 us
    all_gather x2 -> x0, waiting for transfers between devices: 181 us -> none  [the longest x1 107 us: shards(): full_up = lax.all_gather(up_weight, 'fs', axis=0, tiled=True)]
    all_gather x0 -> x1, blocking collectives: none -> 102 us  [shards(): lax.all_gather(packed.astype(jnp.float16), 'fs', axis=0, tiled=False)]
    reduce_scatter x1 -> x0, waiting for transfers between devices: 49.9 us -> none  [shards(): lax.psum_scatter(partial_terms.astype(jnp.bfloat16), 'tp', scatter_dimens...]
    ppermute x0 -> x8, starting transfers between devices: none -> 29.5 us  [the longest x3 16 us: shards(): from_right = lax.ppermute(to_left, 'tp', left)]
    ppermute x0 -> x8, waiting for transfers between devices: none -> 22.2 us  [the longest x3 12.8 us: shards(): from_left = lax.ppermute(to_right, 'tp', right)]
    dot_general x1 -> x0, matrix products: 12.1 us -> none  [shards(): jnp.dot(hidden, full_down, preferred_element_type=jnp.float32)]
    pallas_call x0 -> x6, Pallas kernels: none -> 10.5 us  [the longest x2 5.13 us: first(): pl.pallas_call(first_kernel, grid=(1,), in_specs=[pl.BlockSpec((rows, wid...]
    convert_element_type x0 -> x11, other arithmetic: none -> 4.05 us  [the longest x1 1.32 us: shards(): everything[:, :up_rows].astype(jnp.bfloat16).reshape(fs * up_rows, LANES)]
  transfers between devices with their start and end apart: 3 -> 8, of which waited for: 3 -> 6; matrix products, arithmetic and copies ran while one was open for 1% -> 1% of each run, Pallas kernels for 0% -> 3%
where the time goes in v2:
time: 184 us
  blocking collectives  115 us (62%)
  starting transfers between devices  29.5 us (16%)
  waiting for transfers between devices  22.2 us (12%)
  Pallas kernels  10.5 us (6%)
  other arithmetic  6.53 us (4%)
    all_gather x1, blocking collectives, shards(): lax.all_gather(packed.astype(jnp.float16), 'fs', axis=0, tiled=False)  102 us
    ppermute x3, starting transfers between devices, shards(): from_right = lax.ppermute(to_left, 'tp', left)  16 us
    ppermute x3, waiting for transfers between devices, shards(): from_left = lax.ppermute(to_right, 'tp', right)  12.8 us
    all_to_all x1, blocking collectives, from_everyone(): return lax.all_to_all(copies, axis, split_axis=0, concat_axis=0, tiled=True)  12.6 us
    ppermute x1, waiting for transfers between devices, shards(): from_left = lax.ppermute(top_part, 'tp', right)  6.76 us
    ppermute x3, starting transfers between devices, shards(): from_left = lax.ppermute(to_right, 'tp', right)  5.85 us
    ppermute x1, starting transfers between devices, shards(): from_right = lax.ppermute(bottom_part, 'tp', left)  5.76 us
    pallas_call x2, Pallas kernels, first(): pl.pallas_call(first_kernel, grid=(1,), in_specs=[pl.BlockSpec((rows, wid...  5.13 us
  transfers between devices with their start and end apart: 8, of which 6 were waited for; matrix products, arithmetic and copies ran while one was open for 1% of the time, Pallas kernels for 3%

profile of v2, /device:TPU:80, one launch (start us, length us, event | category | flops | bytes accessed | tf_op | source)
XLA Modules:
  0.0 184.0 jit_solution(5434360395299860529)
XLA Ops:
  0.0 1.2 and_select_fusion.order_ref
  1.2 2.0 %pack.1 = bf16[136,1024]{1,0:T(8,128)(2,1)} custom-call(s32[8]{0:T(128)} %and_select_fusion.order_ref, bf16[64,1024]{1,0:T(8,128)(2,1)} %up_ref.1, bf16[32,2048]{1,0:T(8,128)(2,1)} %down_ref.1), custom_call_target="tpu_custom_call" | custom-call | tf_op jit(solution)/shard_map/pack/pallas_call | solution.py:68
  3.2 1.0 convert_element_type.108
  4.2 101.9 %all-gather.2 = f16[4352,1024]{1,0:T(8,128)(2,1)S(1)} all-gather(f16[136,1024]{1,0:T(8,128)(2,1)S(1)} %convert_element_type.108), channel_id=2, replica_groups=mesh['grp'=2,'fs'=32,'tp'=8] {'fs'}, dimensions={0}, use_global_device_ids=true | all-gather | bytes 9191424 | tf_op jit(solution)/shard_map/all_gather | solution.py:174
  106.1 0.2 slice_convert_fusion.3
  106.2 0.0 copy-start
  106.3 0.0 copy-start.1
  106.3 1.3 slice_convert_fusion
  107.6 0.5 copy-done
  108.1 0.0 copy-done.1
  108.1 2.6 %first.3 = (bf16[384,1024]{1,0:T(8,128)(2,1)S(1)}, bf16[384,256]{1,0:T(8,128)(2,1)S(1)}) custom-call(bf16[768,2048]{1,0:T(8,128)(2,1)S(1)} %copy-done, f32[1,2048]{1,0:T(1,128)S(1)} %bitcast.53, bf16[2048,1024]{1,0:T(8,128)(2,1)S(1)} %bitcast.46, bf16[32,8,128]{2,1,0:T(8,128)(2,1)S(1)} %slice_convert_fusion.5.inverse_ref, bf16[1024,256]{1,0:T(8,128)(2,1)S(1)} %bitcast.49), custom_call_target="tpu_custom_call" | custom-call | tf_op jit(solution)/shard_map/first/pallas_call | solution.py:114
  110.7 5.8 %collective-permute-start.4 = (bf16[384,256]{1,0:T(8,128)(2,1)S(1)}, bf16[384,256]{1,0:T(8,128)(2,1)S(1)}, u32[]{:S(2)}, u32[]{:S(2)}) collective-permute-start(bf16[384,256]{1,0:T(8,128)(2,1)S(1)} %get-tuple-element.18), channel_id=1, source_target_pairs={{0,7},{1,0},{2,1},{3,2},{4,3},{5,4},{6,5},{7,6},{8,15},{9,8},{10,9... | collective-permute-start | bytes 589832 | tf_op jit(solution)/shard_map/ppermute | solution.py:196
  116.5 2.6 %first.2 = (bf16[384,1024]{1,0:T(8,128)(2,1)S(1)}, bf16[384,256]{1,0:T(8,128)(2,1)S(1)}) custom-call(bf16[768,2048]{1,0:T(8,128)(2,1)S(1)} %copy-done, f32[1,2048]{1,0:T(1,128)S(1)} %bitcast.54, bf16[2048,1024]{1,0:T(8,128)(2,1)S(1)} %bitcast.47, bf16[32,8,128]{2,1,0:T(8,128)(2,1)S(1)} %slice_convert_fusion.5.inverse_ref, bf16[1024,256]{1,0:T(8,128)(2,1)S(1)} %bitcast.50), custom_call_target="tpu_custom_call" | custom-call | tf_op jit(solution)/shard_map/first/pallas_call | solution.py:114
  119.1 2.0 %collective-permute-start = (bf16[384,256]{1,0:T(8,128)(2,1)S(1)}, bf16[384,256]{1,0:T(8,128)(2,1)S(1)}, u32[]{:S(2)}, u32[]{:S(2)}) collective-permute-start(bf16[384,256]{1,0:T(8,128)(2,1)S(1)} %get-tuple-element.16), channel_id=1, source_target_pairs={{0,1},{1,2},{2,3},{3,4},{4,5},{5,6},{6,7},{7,0},{8,9},{9,10},{10,1... | collective-permute-start | bytes 589832 | tf_op jit(solution)/shard_map/ppermute | solution.py:195
  121.0 0.3 slice_convert_fusion.2
  121.3 1.0 rest.3
  122.3 0.0 collective-permute-done.4
  122.3 6.8 %collective-permute-done = bf16[384,256]{1,0:T(8,128)(2,1)S(1)} collective-permute-done((bf16[384,256]{1,0:T(8,128)(2,1)S(1)}, bf16[384,256]{1,0:T(8,128)(2,1)S(1)}, u32[]{:S(2)}, u32[]{:S(2)}) %collective-permute-start) | collective-permute-done | bytes 196640 | tf_op jit(solution)/shard_map/ppermute | solution.py:195
  129.1 0.1 fusion.6
  129.2 2.0 %collective-permute-start.1 = (bf16[768,256]{1,0:T(8,128)(2,1)S(1)}, bf16[768,256]{1,0:T(8,128)(2,1)S(1)}, u32[]{:S(2)}, u32[]{:S(2)}) collective-permute-start(bf16[768,256]{1,0:T(8,128)(2,1)S(1)} %pad_maximum_fusion), channel_id=1, source_target_pairs={{0,1},{1,2},{2,3},{3,4},{4,5},{5,6},{6,7},{7,0},{8,9},{9,10},{10,1... | collective-permute-start | bytes 1179656 | tf_op jit(solution)/shard_map/ppermute | solution.py:210
  131.2 5.2 %collective-permute-start.5 = (bf16[768,256]{1,0:T(8,128)(2,1)S(1)}, bf16[768,256]{1,0:T(8,128)(2,1)S(1)}, u32[]{:S(2)}, u32[]{:S(2)}) collective-permute-start(bf16[768,256]{1,0:T(8,128)(2,1)S(1)} %pad_maximum_fusion.1), channel_id=1, source_target_pairs={{0,7},{1,0},{2,1},{3,2},{4,3},{5,4},{6,5},{7,6},{8,15},{9,8},{10,9... | collective-permute-start | bytes 1179656 | tf_op jit(solution)/shard_map/ppermute | solution.py:211
  136.4 0.6 slice_convert_fusion.1
  137.0 1.8 rest.4
  138.9 0.2 slice_convert_fusion.4
  139.0 0.0 copy-start.2
  139.0 0.6 rest.5
  139.6 3.0 %collective-permute-done.1 = bf16[768,256]{1,0:T(8,128)(2,1)S(1)} collective-permute-done((bf16[768,256]{1,0:T(8,128)(2,1)S(1)}, bf16[768,256]{1,0:T(8,128)(2,1)S(1)}, u32[]{:S(2)}, u32[]{:S(2)}) %collective-permute-start.1) | collective-permute-done | bytes 393248 | tf_op jit(solution)/shard_map/ppermute | solution.py:210
  142.6 0.1 fusion.3
  142.7 2.0 %collective-permute-start.2 = (bf16[768,256]{1,0:T(8,128)(2,1)S(1)}, bf16[768,256]{1,0:T(8,128)(2,1)S(1)}, u32[]{:S(2)}, u32[]{:S(2)}) collective-permute-start(bf16[768,256]{1,0:T(8,128)(2,1)S(1)} %fusion.3), channel_id=1, source_target_pairs={{0,1},{1,2},{2,3},{3,4},{4,5},{5,6},{6,7},{7,0},{8,9},{9,10},{10,1... | collective-permute-start | bytes 1179656 | tf_op jit(solution)/shard_map/ppermute | solution.py:210
  144.7 0.0 collective-permute-done.5
  144.7 0.1 fusion.1
  144.8 5.2 %collective-permute-start.6 = (bf16[768,256]{1,0:T(8,128)(2,1)S(1)}, bf16[768,256]{1,0:T(8,128)(2,1)S(1)}, u32[]{:S(2)}, u32[]{:S(2)}) collective-permute-start(bf16[768,256]{1,0:T(8,128)(2,1)S(1)} %fusion.1), channel_id=1, source_target_pairs={{0,7},{1,0},{2,1},{3,2},{4,3},{5,4},{6,5},{7,6},{8,15},{9,8},{10,9... | collective-permute-start | bytes 1179656 | tf_op jit(solution)/shard_map/ppermute | solution.py:211
  150.0 5.3 %collective-permute-done.2 = bf16[768,256]{1,0:T(8,128)(2,1)S(1)} collective-permute-done((bf16[768,256]{1,0:T(8,128)(2,1)S(1)}, bf16[768,256]{1,0:T(8,128)(2,1)S(1)}, u32[]{:S(2)}, u32[]{:S(2)}) %collective-permute-start.2) | collective-permute-done | bytes 393248 | tf_op jit(solution)/shard_map/ppermute | solution.py:210
  155.3 1.3 collective-permute-done.6
  156.6 0.2 fusion.2
  156.8 2.0 %collective-permute-start.3 = (bf16[768,256]{1,0:T(8,128)(2,1)S(1)}, bf16[768,256]{1,0:T(8,128)(2,1)S(1)}, u32[]{:S(2)}, u32[]{:S(2)}) collective-permute-start(bf16[768,256]{1,0:T(8,128)(2,1)S(1)} %get-tuple-element.19), channel_id=1, source_target_pairs={{0,1},{1,2},{2,3},{3,4},{4,5},{5,6},{6,7},{7,0},{8,9},{9,10},{10,1... | collective-permute-start | bytes 1179656 | tf_op jit(solution)/shard_map/ppermute | solution.py:210
  158.8 5.6 %collective-permute-start.7 = (bf16[768,256]{1,0:T(8,128)(2,1)S(1)}, bf16[768,256]{1,0:T(8,128)(2,1)S(1)}, u32[]{:S(2)}, u32[]{:S(2)}) collective-permute-start(bf16[768,256]{1,0:T(8,128)(2,1)S(1)} %get-tuple-element.20), channel_id=1, source_target_pairs={{0,7},{1,0},{2,1},{3,2},{4,3},{5,4},{6,5},{7,6},{8,15},{9,8},{10,9... | collective-permute-start | bytes 1179656 | tf_op jit(solution)/shard_map/ppermute | solution.py:211
  164.4 4.6 %collective-permute-done.3 = bf16[768,256]{1,0:T(8,128)(2,1)S(1)} collective-permute-done((bf16[768,256]{1,0:T(8,128)(2,1)S(1)}, bf16[768,256]{1,0:T(8,128)(2,1)S(1)}, u32[]{:S(2)}, u32[]{:S(2)}) %collective-permute-start.3) | collective-permute-done | bytes 393248 | tf_op jit(solution)/shard_map/ppermute | solution.py:210
  168.9 1.2 collective-permute-done.7
  170.2 0.2 multiply_reduce_fusion
  170.4 12.6 %all_to_all.6 = f32[8,1,768]{2,1,0:T(1,128)S(1)} all-to-all(f32[8,1,768]{2,1,0:T(1,128)S(1)} %broadcast_in_dim.2), channel_id=1, replica_groups=mesh['grp'=2,'fs'=32,'tp'=8] {'tp'}, dimensions={0} | all-to-all | bytes 49152 | tf_op jit(solution)/shard_map/all_to_all | solution.py:18
  183.1 0.0 copy-done.2
  183.1 0.9 multiply_convert_fusion
  (7 shorter events, 0.2 us)
Async XLA Ops:
  106.2 1.9 %copy-start = (bf16[768,2048]{1,0:T(8,128)(2,1)S(1)}, bf16[768,2048]{1,0:T(8,128)(2,1)}, u32[]{:S(2)}) copy-start(bf16[768,2048]{1,0:T(8,128)(2,1)} %x_ref.3) | copy-start | bytes 9437188
  106.3 1.9 %copy-start.1 = (f32[2048]{0:T(1024)S(1)}, f32[2048]{0:T(1024)}, u32[]{:S(2)}) copy-start(f32[2048]{0:T(1024)} %param.7) | copy-start | bytes 24580
  110.7 11.6 %collective-permute-start.4 = (bf16[384,256]{1,0:T(8,128)(2,1)S(1)}, bf16[384,256]{1,0:T(8,128)(2,1)S(1)}, u32[]{:S(2)}, u32[]{:S(2)}) collective-permute-start(bf16[384,256]{1,0:T(8,128)(2,1)S(1)} %get-tuple-element.18), channel_id=1, source_target_pairs={{0,7},{1,0},{2,1},{3,2},{4,3},{5,4},{6,5},{7,6},{8,15},{9,8},{10,9... | collective-permute-start | bytes 589832 | tf_op jit(solution)/shard_map/ppermute | solution.py:196
  119.1 10.0 %collective-permute-start = (bf16[384,256]{1,0:T(8,128)(2,1)S(1)}, bf16[384,256]{1,0:T(8,128)(2,1)S(1)}, u32[]{:S(2)}, u32[]{:S(2)}) collective-permute-start(bf16[384,256]{1,0:T(8,128)(2,1)S(1)} %get-tuple-element.16), channel_id=1, source_target_pairs={{0,1},{1,2},{2,3},{3,4},{4,5},{5,6},{6,7},{7,0},{8,9},{9,10},{10,1... | collective-permute-start | bytes 589832 | tf_op jit(solution)/shard_map/ppermute | solution.py:195
  129.2 13.4 %collective-permute-start.1 = (bf16[768,256]{1,0:T(8,128)(2,1)S(1)}, bf16[768,256]{1,0:T(8,128)(2,1)S(1)}, u32[]{:S(2)}, u32[]{:S(2)}) collective-permute-start(bf16[768,256]{1,0:T(8,128)(2,1)S(1)} %pad_maximum_fusion), channel_id=1, source_target_pairs={{0,1},{1,2},{2,3},{3,4},{4,5},{5,6},{6,7},{7,0},{8,9},{9,10},{10,1... | collective-permute-start | bytes 1179656 | tf_op jit(solution)/shard_map/ppermute | solution.py:210
  131.2 13.5 %collective-permute-start.5 = (bf16[768,256]{1,0:T(8,128)(2,1)S(1)}, bf16[768,256]{1,0:T(8,128)(2,1)S(1)}, u32[]{:S(2)}, u32[]{:S(2)}) collective-permute-start(bf16[768,256]{1,0:T(8,128)(2,1)S(1)} %pad_maximum_fusion.1), channel_id=1, source_target_pairs={{0,7},{1,0},{2,1},{3,2},{4,3},{5,4},{6,5},{7,6},{8,15},{9,8},{10,9... | collective-permute-start | bytes 1179656 | tf_op jit(solution)/shard_map/ppermute | solution.py:211
  139.0 44.0 %copy-start.2 = (f32[256]{0:T(256)S(1)}, f32[256]{0:T(256)}, u32[]{:S(2)}) copy-start(f32[256]{0:T(256)} %param.10) | copy-start | bytes 3076
  142.7 12.5 %collective-permute-start.2 = (bf16[768,256]{1,0:T(8,128)(2,1)S(1)}, bf16[768,256]{1,0:T(8,128)(2,1)S(1)}, u32[]{:S(2)}, u32[]{:S(2)}) collective-permute-start(bf16[768,256]{1,0:T(8,128)(2,1)S(1)} %fusion.3), channel_id=1, source_target_pairs={{0,1},{1,2},{2,3},{3,4},{4,5},{5,6},{6,7},{7,0},{8,9},{9,10},{10,1... | collective-permute-start | bytes 1179656 | tf_op jit(solution)/shard_map/ppermute | solution.py:210
  144.8 11.8 %collective-permute-start.6 = (bf16[768,256]{1,0:T(8,128)(2,1)S(1)}, bf16[768,256]{1,0:T(8,128)(2,1)S(1)}, u32[]{:S(2)}, u32[]{:S(2)}) collective-permute-start(bf16[768,256]{1,0:T(8,128)(2,1)S(1)} %fusion.1), channel_id=1, source_target_pairs={{0,7},{1,0},{2,1},{3,2},{4,3},{5,4},{6,5},{7,6},{8,15},{9,8},{10,9... | collective-permute-start | bytes 1179656 | tf_op jit(solution)/shard_map/ppermute | solution.py:211
  156.8 12.1 %collective-permute-start.3 = (bf16[768,256]{1,0:T(8,128)(2,1)S(1)}, bf16[768,256]{1,0:T(8,128)(2,1)S(1)}, u32[]{:S(2)}, u32[]{:S(2)}) collective-permute-start(bf16[768,256]{1,0:T(8,128)(2,1)S(1)} %get-tuple-element.19), channel_id=1, source_target_pairs={{0,1},{1,2},{2,3},{3,4},{4,5},{5,6},{6,7},{7,0},{8,9},{9,10},{10,1... | collective-permute-start | bytes 1179656 | tf_op jit(solution)/shard_map/ppermute | solution.py:210
  158.8 11.4 %collective-permute-start.7 = (bf16[768,256]{1,0:T(8,128)(2,1)S(1)}, bf16[768,256]{1,0:T(8,128)(2,1)S(1)}, u32[]{:S(2)}, u32[]{:S(2)}) collective-permute-start(bf16[768,256]{1,0:T(8,128)(2,1)S(1)} %get-tuple-element.20), channel_id=1, source_target_pairs={{0,7},{1,0},{2,1},{3,2},{4,3},{5,4},{6,5},{7,6},{8,15},{9,8},{10,9... | collective-permute-start | bytes 1179656 | tf_op jit(solution)/shard_map/ppermute | solution.py:211

commit v3 on v0

v3 whole, which is shorter than its diff:
```python
import functools

import jax
import jax.numpy as jnp
from jax import lax
from jax.experimental import pallas as pl
from jax.experimental.pallas import tpu as pltpu
from jax.sharding import PartitionSpec as P

TOP = 2.0 ** 15
UP_FACTORS = 3
DOWN_FACTORS = 5


def from_everyone(value, axis):
    copies = jnp.broadcast_to(value, (lax.axis_size(axis), *value.shape))
    return lax.all_to_all(copies, axis, split_axis=0, concat_axis=0, tiled=True)


def of_everyone(value, axis):
    everything = from_everyone(value, axis)
    return jnp.sum(everything, axis=0)


def power_factors(top, count):
    factors = []
    for _ in range(count):
        factor = jnp.ones_like(top)
        for power in (8, 4, 2):
            factor = jnp.where(top * factor * 2.0**power <= TOP, factor * 2.0**power, factor)
        for power in (8, 4, 2):
            factor = jnp.where(top * factor > TOP * 2.0 ** (power - 2), factor * 2.0**-power, factor)
        top = top * factor
        factors.append(factor)
    return factors


def largest(value):
    return jnp.max(jnp.max(jnp.abs(value), axis=0, keepdims=True), axis=1, keepdims=True)


def pack_kernel(up_hbm, down_hbm, out_ref, up_ref, down_ref, sems, *, offsets):
    fetches = [
        pltpu.make_async_copy(source, target, sems.at[i])
        for i, (source, target) in enumerate(((up_hbm, up_ref), (down_hbm, down_ref)))
    ]
    for fetch in fetches:
        fetch.start()
    own = out_ref.shape[1]
    up_rows = up_ref.shape[0]
    down_rows = down_ref.shape[0]
    fetches[0].wait()
    up = up_ref[...].astype(jnp.float32)
    up_factors = power_factors(jnp.broadcast_to(largest(up), (1, own)), UP_FACTORS)
    at = 0
    for j in range(up_ref.shape[1] // own):
        piece = up[:, j * own:(j + 1) * own]
        for factor in up_factors:
            piece = piece * factor
        out_ref[at:at + up_rows, :] = piece.astype(jnp.bfloat16)
        at += up_rows
    fetches[1].wait()
    top = largest(down_ref[...].astype(jnp.float32))
    down_factors = power_factors(jnp.broadcast_to(top, (1, own)), DOWN_FACTORS)
    for offset in offsets:
        start = pl.multiple_of((lax.axis_index("tp") + offset) % len(offsets) * own, own)
        piece = down_ref[:, pl.ds(start, own)].astype(jnp.float32)
        for factor in down_factors:
            piece = piece * factor
        out_ref[at:at + down_rows, :] = piece.astype(jnp.bfloat16)
        at += down_rows
    inverses = [1.0 / factor for factor in up_factors + down_factors]
    out_ref[at:, :] = jnp.concatenate(inverses, axis=0).astype(jnp.bfloat16)


def pack(up_weight, down_weight, own, offsets):
    rows = (up_weight.size + down_weight.size) // own + UP_FACTORS + DOWN_FACTORS
    hbm = pl.BlockSpec(memory_space=pltpu.HBM)
    return pl.pallas_call(
        functools.partial(pack_kernel, offsets=offsets),
        in_specs=[hbm, hbm],
        out_shape=jax.ShapeDtypeStruct((rows, own), jnp.bfloat16),
        scratch_shapes=[
            pltpu.VMEM(up_weight.shape, jnp.bfloat16),
            pltpu.VMEM(down_weight.shape, jnp.bfloat16),
            pltpu.SemaphoreType.DMA((2,)),
        ],
        compiler_params=pltpu.CompilerParams(vmem_limit_bytes=8 * 1024 * 1024),
        name="pack",
    )(up_weight, down_weight)


def first_kernel(x_ref, gain_ref, up_ref, inverse_ref, down_ref, hidden_ref, part_ref, up_scale, down_scale):
    shards, _, own = inverse_ref.shape
    up_rows = x_ref.shape[1] // shards

    @pl.when(pl.program_id(0) == 0)
    def _():
        for scale, first, count in ((up_scale, 0, UP_FACTORS), (down_scale, UP_FACTORS, DOWN_FACTORS)):
            per = scale.shape[1] // shards
            for p in range(scale.shape[1] // own):
                owner = (lax.broadcasted_iota(jnp.int32, (1, own), 1) + p * own) // per
                total = jnp.zeros((1, own), jnp.float32)
                for s in range(p * own // per, ((p + 1) * own - 1) // per + 1):
                    rows = inverse_ref[s].astype(jnp.float32)
                    value = rows[first:first + 1]
                    for t in range(1, count):
                        value = value * rows[first + t:first + t + 1]
                    total = jnp.where(owner == s, value, total)
                scale[:, p * own:(p + 1) * own] = total

    x = x_ref[...].astype(jnp.float32)
    factor = lax.rsqrt(jnp.mean(x * x, axis=1, keepdims=True) + 1e-6)
    normed = (x * factor * gain_ref[...]).astype(jnp.bfloat16) * up_scale[...].astype(jnp.bfloat16)
    for q in range(hidden_ref.shape[1] // own):
        weights = up_ref[:, q * up_rows:(q + 1) * up_rows, :].reshape(x_ref.shape[1], own)
        span = slice(q * own, (q + 1) * own)
        up = jnp.dot(normed, weights, preferred_element_type=jnp.float32)
        hidden_ref[:, span] = (jnp.square(jnp.maximum(up, 0.0)) * down_scale[:, span]).astype(jnp.bfloat16)
    down = down_ref[...].reshape(hidden_ref.shape[1], own)
    part_ref[...] = jnp.dot(hidden_ref[...], down, preferred_element_type=jnp.float32).astype(jnp.bfloat16)


def first(tokens, gain, up, inverses, down, rows):
    count, width = tokens.shape
    shards, _, own = down.shape
    hidden = shards * down.shape[1]
    whole = lambda *shape: pl.BlockSpec(shape, lambda i: (0,) * len(shape))
    return pl.pallas_call(
        first_kernel,
        grid=(count // rows,),
        in_specs=[
            pl.BlockSpec((rows, width), lambda i: (i, 0)),
            whole(1, width),
            whole(*up.shape),
            whole(*inverses.shape),
            whole(*down.shape),
        ],
        out_specs=[pl.BlockSpec((rows, hidden), lambda i: (i, 0)), pl.BlockSpec((rows, own), lambda i: (i, 0))],
        out_shape=[
            jax.ShapeDtypeStruct((count, hidden), jnp.bfloat16),
            jax.ShapeDtypeStruct((count, own), jnp.bfloat16),
        ],
        scratch_shapes=[pltpu.VMEM((1, width), jnp.float32), pltpu.VMEM((1, hidden), jnp.float32)],
        compiler_params=pltpu.CompilerParams(vmem_limit_bytes=20 * 1024 * 1024),
        name="first",
    )(tokens, gain.reshape(1, width), up, inverses, down)


def rest_kernel(hidden_ref, down_ref, *out_refs):
    width = hidden_ref.shape[1]
    rows = width // down_ref.shape[0]
    for j, out_ref in enumerate(out_refs):
        own = out_ref.shape[1]
        paired = j < len(out_refs) // 2 * 2
        block = (j + lax.axis_index("fs")) % 2 + j // 2 * 2 if paired else j
        start = pl.multiple_of(block * rows, rows)
        down = down_ref[:, pl.ds(start, rows), :].reshape(width, own)
        out_ref[...] = jnp.dot(hidden_ref[...], down, preferred_element_type=jnp.float32).astype(jnp.bfloat16)


def rest(hidden, down):
    shards, rows, own = down.shape
    count = rows // (hidden.shape[1] // shards)
    vmem = pl.BlockSpec(memory_space=pltpu.VMEM)
    return pl.pallas_call(
        rest_kernel,
        in_specs=[vmem, vmem],
        out_specs=[vmem] * count,
        out_shape=[jax.ShapeDtypeStruct((hidden.shape[0], own), jnp.bfloat16)] * count,
        compiler_params=pltpu.CompilerParams(vmem_limit_bytes=8 * 1024 * 1024),
        name="rest",
    )(hidden, down)


def add(a, b):
    return (a.astype(jnp.float32) + b.astype(jnp.float32)).astype(jnp.bfloat16)


def shards(tokens, pre_gain, up_weight, down_weight, post_gain):
    eps = 1e-06
    fs = lax.axis_size("fs")
    tp = lax.axis_size("tp")
    own = post_gain.shape[0]
    up_rows = up_weight.size // own
    down_rows = down_weight.shape[0]
    offsets = [tp // 2]
    for distance in range(tp // 2 - 1, 0, -1):
        offsets += [distance, tp - distance]
    offsets.append(0)
    packed = pack(up_weight, down_weight, own, offsets)
    everything = lax.all_gather(packed.astype(jnp.float16), "fs", axis=0, tiled=False)

    def down(source, start, stop):
        return source[:, up_rows + start * down_rows:up_rows + stop * down_rows].astype(jnp.bfloat16)

    up = everything[:, :up_rows].astype(jnp.bfloat16)
    inverses = everything[:, up_rows + tp * down_rows:].astype(jnp.bfloat16)
    hidden, one = first(tokens, pre_gain, up, inverses, down(everything, 0, 1), tokens.shape[0] // 2)

    def send(value, sign):
        pairs = []
        for f in range(fs):
            step = sign if f % 2 == 0 else -sign
            pairs += [(f * tp + t, f * tp + (t + step) % tp) for t in range(tp)]
        return lax.ppermute(value, ("fs", "tp"), pairs)

    one = send(one, 1)
    held, hidden = lax.optimization_barrier((everything, hidden))
    *parts, own_part = rest(hidden, down(held, 1, tp))
    two = send(parts[1], -1)
    one = send(add(one, parts[0]), 1)
    for step in range(1, tp // 2 - 1):
        two = send(add(two, parts[2 * step + 1]), -1)
        one = send(add(one, parts[2 * step]), 1)
    mixed = own_part.astype(jnp.float32) + one.astype(jnp.float32) + two.astype(jnp.float32)
    squares = of_everyone(jnp.sum(mixed * mixed, axis=1), "tp")
    factor = lax.rsqrt(squares / (tp * own) + eps)
    return (mixed * factor[:, None] * post_gain).astype(jnp.bfloat16)


def solution(mesh):
    in_specs = (P(("grp", "fs"), None), P(), P("fs", "tp"), P(("tp", "fs"), None), P("tp"))
    out_specs = P(("grp", "fs"), "tp")
    return jax.shard_map(shards, mesh=mesh, in_specs=in_specs, out_specs=out_specs, check_vma=False)
```

time: 277 us -> 177 us (0.64)
  waiting for transfers between devices: 233 us -> 19.1 us
  blocking collectives: 12.8 us -> 119 us
  starting transfers between devices: 0.12 us -> 23.3 us
  between operations: 13.2 us -> 0.19 us
  matrix products: 12.1 us -> 0 us
  Pallas kernels: 0 us -> 8.87 us
  local copies, waits for them, and re-layouts: 0.02 us -> 2.85 us
    all_gather x2 -> x0, waiting for transfers between devices: 181 us -> none  [the longest x1 107 us: shards(): full_up = lax.all_gather(up_weight, 'fs', axis=0, tiled=True)]
    all_gather x0 -> x1, blocking collectives: none -> 100 us  [shards(): lax.all_gather(packed.astype(jnp.float16), 'fs', axis=0, tiled=False)]
    reduce_scatter x1 -> x0, waiting for transfers between devices: 49.9 us -> none  [shards(): lax.psum_scatter(partial_terms.astype(jnp.bfloat16), 'tp', scatter_dimens...]
    ppermute x0 -> x7, starting transfers between devices: none -> 23.3 us  [send(): return lax.ppermute(value, ('fs', 'tp'), pairs)]
    ppermute x0 -> x7, waiting for transfers between devices: none -> 19.1 us  [send(): return lax.ppermute(value, ('fs', 'tp'), pairs)]
    dot_general x1 -> x0, matrix products: 12.1 us -> none  [shards(): jnp.dot(hidden, full_down, preferred_element_type=jnp.float32)]
    pallas_call x0 -> x3, Pallas kernels: none -> 8.87 us  [the longest x1 5.12 us: first(): pl.pallas_call(first_kernel, grid=(count // rows,), in_specs=[pl.BlockSpe...]
    all_to_all x1, blocking collectives: 12.8 us -> 19 us  [from_everyone(): return lax.all_to_all(copies, axis, split_axis=0, concat_axis=0, tiled=True)]
  transfers between devices with their start and end apart: 3 -> 7, of which waited for: 3 -> 5; matrix products, arithmetic and copies ran while one was open for 1% -> 1% of each run, Pallas kernels for 0% -> 2%
where the time goes in v3:
time: 177 us
  blocking collectives  119 us (67%)
  starting transfers between devices  23.3 us (13%)
  waiting for transfers between devices  19.1 us (11%)
  Pallas kernels  8.87 us (5%)
  other arithmetic  3.52 us (2%)
  local copies, waits for them, and re-layouts  2.85 us (2%)
    all_gather x1, blocking collectives, shards(): lax.all_gather(packed.astype(jnp.float16), 'fs', axis=0, tiled=False)  100 us
    ppermute x7, starting transfers between devices, send(): return lax.ppermute(value, ('fs', 'tp'), pairs)  23.3 us
    ppermute x7, waiting for transfers between devices, send(): return lax.ppermute(value, ('fs', 'tp'), pairs)  19.1 us
    all_to_all x1, blocking collectives, from_everyone(): return lax.all_to_all(copies, axis, split_axis=0, concat_axis=0, tiled=True)  19 us
    pallas_call x1, Pallas kernels, first(): pl.pallas_call(first_kernel, grid=(count // rows,), in_specs=[pl.BlockSpe...  5.12 us
  transfers between devices with their start and end apart: 7, of which 5 were waited for; matrix products, arithmetic and copies ran while one was open for 1% of the time, Pallas kernels for 2%

profile of v3, /device:TPU:80, one launch (start us, length us, event | category | flops | bytes accessed | tf_op | source)
XLA Modules:
  0.0 177.0 jit_solution(2232952982350323596)
XLA Ops:
  0.0 0.0 copy-start.1
  0.0 0.9 copy-done.1
  0.9 0.0 copy-start.2
  0.9 0.9 copy-done.2
  1.8 0.7 pack.1
  2.6 100.1 %all-gather.2 = f16[16640,256]{1,0:T(8,128)(2,1)S(1)} all-gather(f16[520,256]{1,0:T(8,128)(2,1)S(1)} %convert_element_type.72), channel_id=2, replica_groups=mesh['grp'=2,'fs'=32,'tp'=8] {'fs'}, dimensions={0}, use_global_device_ids=true | all-gather | bytes 8785920 | tf_op jit(solution)/shard_map/all_gather | solution.py:192
  102.7 0.1 slice_convert_fusion.2.down_ref
  102.8 0.0 copy-start
  102.8 0.0 copy-start.3
  102.8 0.8 slice_convert_fusion.up_ref
  103.7 1.0 copy-done
  104.7 0.0 copy-done.3
  104.7 5.1 %first.1 = (bf16[768,1024]{1,0:T(8,128)(2,1)S(1)}, bf16[768,256]{1,0:T(8,128)(2,1)S(1)}) custom-call(bf16[768,2048]{1,0:T(8,128)(2,1)S(1)} %copy-done, f32[1,2048]{1,0:T(1,128)S(1)} %bitcast.2, bf16[32,256,256]{2,1,0:T(8,128)(2,1)S(1)} %slice_convert_fusion.up_ref, bf16[32,8,256]{2,1,0:T(8,128)(2,1)S(1)} %slice_convert_fusion.3.inverse_ref, ...), custom_call_target="tpu_custom_call" | custom-call | tf_op jit(solution)/shard_map/first/pallas_call | solution.py:129
  109.8 3.6 %collective-permute-start = (bf16[768,256]{1,0:T(8,128)(2,1)S(1)}, bf16[768,256]{1,0:T(8,128)(2,1)S(1)}, u32[]{:S(2)}, u32[]{:S(2)}) collective-permute-start(bf16[768,256]{1,0:T(8,128)(2,1)S(1)} %get-tuple-element.20), channel_id=1, source_target_pairs={{0,1},{1,2},{2,3},{3,4},{4,5},{5,6},{6,7},{7,0},{8,15},{9,8},{10,9... | collective-permute-start | bytes 1179656 | tf_op jit(solution)/shard_map/ppermute | solution.py:206
  113.4 0.7 slice_convert_fusion.1.down_ref
  114.1 3.1 %rest.1 = (bf16[768,256]{1,0:T(8,128)(2,1)S(1)}, bf16[768,256]{1,0:T(8,128)(2,1)S(1)}, bf16[768,256]{1,0:T(8,128)(2,1)S(1)}, bf16[768,256]{1,0:T(8,128)(2,1)S(1)...) custom-call(bf16[768,1024]{1,0:T(8,128)(2,1)S(1)} %get-tuple-element.17.hidden_ref, ...), custom_call_target="tpu_custom_call" | custom-call | tf_op jit(solution)/shard_map/rest/pallas_call | solution.py:166
  117.2 0.0 copy-start.4
  117.2 4.2 %collective-permute-start.4 = (bf16[768,256]{1,0:T(8,128)(2,1)S(1)}, bf16[768,256]{1,0:T(8,128)(2,1)S(1)}, u32[]{:S(2)}, u32[]{:S(2)}) collective-permute-start(bf16[768,256]{1,0:T(8,128)(2,1)S(1)} %get-tuple-element.24), channel_id=1, source_target_pairs={{0,7},{1,0},{2,1},{3,2},{4,3},{5,4},{6,5},{7,6},{8,9},{9,10},{10,1... | collective-permute-start | bytes 1179656 | tf_op jit(solution)/shard_map/ppermute | solution.py:206
  121.4 0.0 collective-permute-done
  121.4 0.1 add_convert_fusion.4
  121.5 2.0 %collective-permute-start.1 = (bf16[768,256]{1,0:T(8,128)(2,1)S(1)}, bf16[768,256]{1,0:T(8,128)(2,1)S(1)}, u32[]{:S(2)}, u32[]{:S(2)}) collective-permute-start(bf16[768,256]{1,0:T(8,128)(2,1)S(1)} %add_convert_fusion.4), channel_id=1, source_target_pairs={{0,1},{1,2},{2,3},{3,4},{4,5},{5,6},{6,7},{7,0},{8,15},{9,8},{10,9... | collective-permute-start | bytes 1179656 | tf_op jit(solution)/shard_map/ppermute | solution.py:206
  123.5 4.3 %collective-permute-done.4 = bf16[768,256]{1,0:T(8,128)(2,1)S(1)} collective-permute-done((bf16[768,256]{1,0:T(8,128)(2,1)S(1)}, bf16[768,256]{1,0:T(8,128)(2,1)S(1)}, u32[]{:S(2)}, u32[]{:S(2)}) %collective-permute-start.4) | collective-permute-done | bytes 393248 | tf_op jit(solution)/shard_map/ppermute | solution.py:206
  127.7 0.1 add_convert_fusion.1
  127.8 4.7 %collective-permute-start.5 = (bf16[768,256]{1,0:T(8,128)(2,1)S(1)}, bf16[768,256]{1,0:T(8,128)(2,1)S(1)}, u32[]{:S(2)}, u32[]{:S(2)}) collective-permute-start(bf16[768,256]{1,0:T(8,128)(2,1)S(1)} %add_convert_fusion.1), channel_id=1, source_target_pairs={{0,7},{1,0},{2,1},{3,2},{4,3},{5,4},{6,5},{7,6},{8,9},{9,10},{10,1... | collective-permute-start | bytes 1179656 | tf_op jit(solution)/shard_map/ppermute | solution.py:206
  132.5 1.1 collective-permute-done.1
  133.7 0.1 add_convert_fusion.3
  133.8 2.0 %collective-permute-start.2 = (bf16[768,256]{1,0:T(8,128)(2,1)S(1)}, bf16[768,256]{1,0:T(8,128)(2,1)S(1)}, u32[]{:S(2)}, u32[]{:S(2)}) collective-permute-start(bf16[768,256]{1,0:T(8,128)(2,1)S(1)} %add_convert_fusion.3), channel_id=1, source_target_pairs={{0,1},{1,2},{2,3},{3,4},{4,5},{5,6},{6,7},{7,0},{8,15},{9,8},{10,9... | collective-permute-start | bytes 1179656 | tf_op jit(solution)/shard_map/ppermute | solution.py:206
  135.7 5.2 %collective-permute-done.5 = bf16[768,256]{1,0:T(8,128)(2,1)S(1)} collective-permute-done((bf16[768,256]{1,0:T(8,128)(2,1)S(1)}, bf16[768,256]{1,0:T(8,128)(2,1)S(1)}, u32[]{:S(2)}, u32[]{:S(2)}) %collective-permute-start.5) | collective-permute-done | bytes 393248 | tf_op jit(solution)/shard_map/ppermute | solution.py:206
  141.0 0.1 add_convert_fusion
  141.1 3.2 %collective-permute-start.6 = (bf16[768,256]{1,0:T(8,128)(2,1)S(1)}, bf16[768,256]{1,0:T(8,128)(2,1)S(1)}, u32[]{:S(2)}, u32[]{:S(2)}) collective-permute-start(bf16[768,256]{1,0:T(8,128)(2,1)S(1)} %add_convert_fusion), channel_id=1, source_target_pairs={{0,7},{1,0},{2,1},{3,2},{4,3},{5,4},{6,5},{7,6},{8,9},{9,10},{10,1... | collective-permute-start | bytes 1179656 | tf_op jit(solution)/shard_map/ppermute | solution.py:206
  144.3 0.7 collective-permute-done.2
  145.1 0.1 add_convert_fusion.2
  145.2 3.8 %collective-permute-start.3 = (bf16[768,256]{1,0:T(8,128)(2,1)S(1)}, bf16[768,256]{1,0:T(8,128)(2,1)S(1)}, u32[]{:S(2)}, u32[]{:S(2)}) collective-permute-start(bf16[768,256]{1,0:T(8,128)(2,1)S(1)} %add_convert_fusion.2), channel_id=1, source_target_pairs={{0,1},{1,2},{2,3},{3,4},{4,5},{5,6},{6,7},{7,0},{8,15},{9,8},{10,9... | collective-permute-start | bytes 1179656 | tf_op jit(solution)/shard_map/ppermute | solution.py:206
  149.0 7.7 %collective-permute-done.6 = bf16[768,256]{1,0:T(8,128)(2,1)S(1)} collective-permute-done((bf16[768,256]{1,0:T(8,128)(2,1)S(1)}, bf16[768,256]{1,0:T(8,128)(2,1)S(1)}, u32[]{:S(2)}, u32[]{:S(2)}) %collective-permute-start.6) | collective-permute-done | bytes 393248 | tf_op jit(solution)/shard_map/ppermute | solution.py:206
  156.8 0.0 collective-permute-done.3
  156.8 0.2 multiply_reduce_fusion
  157.0 19.0 %all_to_all.6 = f32[8,1,768]{2,1,0:T(1,128)S(1)} all-to-all(f32[8,1,768]{2,1,0:T(1,128)S(1)} %broadcast_in_dim.2), channel_id=1, replica_groups=mesh['grp'=2,'fs'=32,'tp'=8] {'tp'}, dimensions={0} | all-to-all | bytes 49152 | tf_op jit(solution)/shard_map/all_to_all | solution.py:17
  176.0 0.0 copy-done.4
  176.0 0.9 multiply_convert_fusion
  (5 shorter events, 0.1 us)
Async XLA Ops:
  0.0 0.9 copy-start.1
  0.9 0.9 copy-start.2
  102.8 1.9 %copy-start = (bf16[768,2048]{1,0:T(8,128)(2,1)S(1)}, bf16[768,2048]{1,0:T(8,128)(2,1)}, u32[]{:S(2)}) copy-start(bf16[768,2048]{1,0:T(8,128)(2,1)} %x_ref.1) | copy-start | bytes 9437188
  102.8 1.9 %copy-start.3 = (f32[2048]{0:T(1024)S(1)}, f32[2048]{0:T(1024)}, u32[]{:S(2)}) copy-start(f32[2048]{0:T(1024)} %param.6) | copy-start | bytes 24580
  109.8 11.6 %collective-permute-start = (bf16[768,256]{1,0:T(8,128)(2,1)S(1)}, bf16[768,256]{1,0:T(8,128)(2,1)S(1)}, u32[]{:S(2)}, u32[]{:S(2)}) collective-permute-start(bf16[768,256]{1,0:T(8,128)(2,1)S(1)} %get-tuple-element.20), channel_id=1, source_target_pairs={{0,1},{1,2},{2,3},{3,4},{4,5},{5,6},{6,7},{7,0},{8,15},{9,8},{10,9... | collective-permute-start | bytes 1179656 | tf_op jit(solution)/shard_map/ppermute | solution.py:206
  117.2 58.8 %copy-start.4 = (f32[256]{0:T(256)S(1)}, f32[256]{0:T(256)}, u32[]{:S(2)}) copy-start(f32[256]{0:T(256)} %param.9) | copy-start | bytes 3076
  117.2 10.5 %collective-permute-start.4 = (bf16[768,256]{1,0:T(8,128)(2,1)S(1)}, bf16[768,256]{1,0:T(8,128)(2,1)S(1)}, u32[]{:S(2)}, u32[]{:S(2)}) collective-permute-start(bf16[768,256]{1,0:T(8,128)(2,1)S(1)} %get-tuple-element.24), channel_id=1, source_target_pairs={{0,7},{1,0},{2,1},{3,2},{4,3},{5,4},{6,5},{7,6},{8,9},{9,10},{10,1... | collective-permute-start | bytes 1179656 | tf_op jit(solution)/shard_map/ppermute | solution.py:206
  121.5 12.2 %collective-permute-start.1 = (bf16[768,256]{1,0:T(8,128)(2,1)S(1)}, bf16[768,256]{1,0:T(8,128)(2,1)S(1)}, u32[]{:S(2)}, u32[]{:S(2)}) collective-permute-start(bf16[768,256]{1,0:T(8,128)(2,1)S(1)} %add_convert_fusion.4), channel_id=1, source_target_pairs={{0,1},{1,2},{2,3},{3,4},{4,5},{5,6},{6,7},{7,0},{8,15},{9,8},{10,9... | collective-permute-start | bytes 1179656 | tf_op jit(solution)/shard_map/ppermute | solution.py:206
  127.8 13.1 %collective-permute-start.5 = (bf16[768,256]{1,0:T(8,128)(2,1)S(1)}, bf16[768,256]{1,0:T(8,128)(2,1)S(1)}, u32[]{:S(2)}, u32[]{:S(2)}) collective-permute-start(bf16[768,256]{1,0:T(8,128)(2,1)S(1)} %add_convert_fusion.1), channel_id=1, source_target_pairs={{0,7},{1,0},{2,1},{3,2},{4,3},{5,4},{6,5},{7,6},{8,9},{9,10},{10,1... | collective-permute-start | bytes 1179656 | tf_op jit(solution)/shard_map/ppermute | solution.py:206
  133.8 11.3 %collective-permute-start.2 = (bf16[768,256]{1,0:T(8,128)(2,1)S(1)}, bf16[768,256]{1,0:T(8,128)(2,1)S(1)}, u32[]{:S(2)}, u32[]{:S(2)}) collective-permute-start(bf16[768,256]{1,0:T(8,128)(2,1)S(1)} %add_convert_fusion.3), channel_id=1, source_target_pairs={{0,1},{1,2},{2,3},{3,4},{4,5},{5,6},{6,7},{7,0},{8,15},{9,8},{10,9... | collective-permute-start | bytes 1179656 | tf_op jit(solution)/shard_map/ppermute | solution.py:206
  141.1 15.7 %collective-permute-start.6 = (bf16[768,256]{1,0:T(8,128)(2,1)S(1)}, bf16[768,256]{1,0:T(8,128)(2,1)S(1)}, u32[]{:S(2)}, u32[]{:S(2)}) collective-permute-start(bf16[768,256]{1,0:T(8,128)(2,1)S(1)} %add_convert_fusion), channel_id=1, source_target_pairs={{0,7},{1,0},{2,1},{3,2},{4,3},{5,4},{6,5},{7,6},{8,9},{9,10},{10,1... | collective-permute-start | bytes 1179656 | tf_op jit(solution)/shard_map/ppermute | solution.py:206
  145.2 11.6 %collective-permute-start.3 = (bf16[768,256]{1,0:T(8,128)(2,1)S(1)}, bf16[768,256]{1,0:T(8,128)(2,1)S(1)}, u32[]{:S(2)}, u32[]{:S(2)}) collective-permute-start(bf16[768,256]{1,0:T(8,128)(2,1)S(1)} %add_convert_fusion.2), channel_id=1, source_target_pairs={{0,1},{1,2},{2,3},{3,4},{4,5},{5,6},{6,7},{7,0},{8,15},{9,8},{10,9... | collective-permute-start | bytes 1179656 | tf_op jit(solution)/shard_map/ppermute | solution.py:206

commit v4 on v3

--- a/solution.py
+++ b/solution.py
@@ -90,7 +90,7 @@
     )(up_weight, down_weight)
 
 
-def first_kernel(x_ref, gain_ref, up_ref, inverse_ref, down_ref, hidden_ref, part_ref, up_scale, down_scale):
+def first_kernel(x_ref, gain_ref, up_ref, inverse_ref, down_ref, hidden_ref, one_ref, two_ref, up_scale, down_scale):
     shards, _, own = inverse_ref.shape
     up_rows = x_ref.shape[1] // shards
 
@@ -117,14 +117,16 @@
         span = slice(q * own, (q + 1) * own)
         up = jnp.dot(normed, weights, preferred_element_type=jnp.float32)
         hidden_ref[:, span] = (jnp.square(jnp.maximum(up, 0.0)) * down_scale[:, span]).astype(jnp.bfloat16)
-    down = down_ref[...].reshape(hidden_ref.shape[1], own)
-    part_ref[...] = jnp.dot(hidden_ref[...], down, preferred_element_type=jnp.float32).astype(jnp.bfloat16)
+    down_rows = hidden_ref.shape[1] // shards
+    for j, part_ref in enumerate((one_ref, two_ref)):
+        down = down_ref[:, j * down_rows:(j + 1) * down_rows, :].reshape(hidden_ref.shape[1], own)
+        part_ref[...] = jnp.dot(hidden_ref[...], down, preferred_element_type=jnp.float32).astype(jnp.bfloat16)
 
 
 def first(tokens, gain, up, inverses, down, rows):
     count, width = tokens.shape
     shards, _, own = down.shape
-    hidden = shards * down.shape[1]
+    hidden = shards * down.shape[1] // 2
     whole = lambda *shape: pl.BlockSpec(shape, lambda i: (0,) * len(shape))
     return pl.pallas_call(
         first_kernel,
@@ -136,41 +138,45 @@
             whole(*inverses.shape),
             whole(*down.shape),
         ],
-        out_specs=[pl.BlockSpec((rows, hidden), lambda i: (i, 0)), pl.BlockSpec((rows, own), lambda i: (i, 0))],
-        out_shape=[
-            jax.ShapeDtypeStruct((count, hidden), jnp.bfloat16),
-            jax.ShapeDtypeStruct((count, own), jnp.bfloat16),
-        ],
+        out_specs=[pl.BlockSpec((rows, columns), lambda i: (i, 0)) for columns in (hidden, own, own)],
+        out_shape=[jax.ShapeDtypeStruct((count, columns), jnp.bfloat16) for columns in (hidden, own, own)],
         scratch_shapes=[pltpu.VMEM((1, width), jnp.float32), pltpu.VMEM((1, hidden), jnp.float32)],
         compiler_params=pltpu.CompilerParams(vmem_limit_bytes=20 * 1024 * 1024),
         name="first",
     )(tokens, gain.reshape(1, width), up, inverses, down)
 
 
-def rest_kernel(hidden_ref, down_ref, *out_refs):
+def rest_kernel(hidden_ref, down_ref, *refs, blocks, turn):
     width = hidden_ref.shape[1]
     rows = width // down_ref.shape[0]
-    for j, out_ref in enumerate(out_refs):
-        own = out_ref.shape[1]
-        paired = j < len(out_refs) // 2 * 2
-        block = (j + lax.axis_index("fs")) % 2 + j // 2 * 2 if paired else j
-        start = pl.multiple_of(block * rows, rows)
-        down = down_ref[:, pl.ds(start, rows), :].reshape(width, own)
-        out_ref[...] = jnp.dot(hidden_ref[...], down, preferred_element_type=jnp.float32).astype(jnp.bfloat16)
-
-
-def rest(hidden, down):
+    mine = lax.axis_index("fs") % 2 == turn
+
+    @pl.when(mine)
+    def _():
+        for j, out_ref in enumerate(refs[-blocks:]):
+            down = down_ref[:, j * rows:(j + 1) * rows, :].reshape(width, out_ref.shape[1])
+            part = jnp.dot(hidden_ref[...], down, preferred_element_type=jnp.float32)
+            out_ref[...] = part.astype(jnp.bfloat16)
+
+    if len(refs) > blocks:
+        @pl.when(jnp.logical_not(mine))
+        def _():
+            for held_ref, out_ref in zip(refs[:blocks], refs[blocks:]):
+                out_ref[...] = held_ref[...]
+
+
+def rest(hidden, down, parts, turn):
     shards, rows, own = down.shape
     count = rows // (hidden.shape[1] // shards)
     vmem = pl.BlockSpec(memory_space=pltpu.VMEM)
     return pl.pallas_call(
-        rest_kernel,
-        in_specs=[vmem, vmem],
+        functools.partial(rest_kernel, blocks=count, turn=turn),
+        in_specs=[vmem] * (2 + len(parts)),
         out_specs=[vmem] * count,
         out_shape=[jax.ShapeDtypeStruct((hidden.shape[0], own), jnp.bfloat16)] * count,
         compiler_params=pltpu.CompilerParams(vmem_limit_bytes=8 * 1024 * 1024),
         name="rest",
-    )(hidden, down)
+    )(hidden, down, *parts)
 
 
 def add(a, b):
@@ -184,8 +190,8 @@
     own = post_gain.shape[0]
     up_rows = up_weight.size // own
     down_rows = down_weight.shape[0]
-    offsets = [tp // 2]
-    for distance in range(tp // 2 - 1, 0, -1):
+    offsets = [tp // 2, tp // 2 + 1, tp // 2 - 1]
+    for distance in range(tp // 2 - 2, 0, -1):
         offsets += [distance, tp - distance]
     offsets.append(0)
     packed = pack(up_weight, down_weight, own, offsets)
@@ -196,21 +202,20 @@
 
     up = everything[:, :up_rows].astype(jnp.bfloat16)
     inverses = everything[:, up_rows + tp * down_rows:].astype(jnp.bfloat16)
-    hidden, one = first(tokens, pre_gain, up, inverses, down(everything, 0, 1), tokens.shape[0] // 2)
-
-    def send(value, sign):
-        pairs = []
-        for f in range(fs):
-            step = sign if f % 2 == 0 else -sign
-            pairs += [(f * tp + t, f * tp + (t + step) % tp) for t in range(tp)]
-        return lax.ppermute(value, ("fs", "tp"), pairs)
-
+    hidden, one, two = first(tokens, pre_gain, up, inverses, down(everything, 0, 2), tokens.shape[0] // 2)
+
+    def send(value, step):
+        return lax.ppermute(value, "tp", [(t, (t + step) % tp) for t in range(tp)])
+
+    held, hidden = lax.optimization_barrier((everything, hidden))
+    rest_down = down(held, 2, tp)
+    parts = rest(hidden, rest_down, [], 0)
+    one, two, *parts = lax.optimization_barrier((one, two, *parts))
     one = send(one, 1)
-    held, hidden = lax.optimization_barrier((everything, hidden))
-    *parts, own_part = rest(hidden, down(held, 1, tp))
-    two = send(parts[1], -1)
-    one = send(add(one, parts[0]), 1)
-    for step in range(1, tp // 2 - 1):
+    two = send(two, -1)
+    part_one, *parts, own_part = rest(hidden, rest_down, parts, 1)
+    one = send(add(one, part_one), 1)
+    for step in range(tp // 2 - 2):
         two = send(add(two, parts[2 * step + 1]), -1)
         one = send(add(one, parts[2 * step]), 1)
     mixed = own_part.astype(jnp.float32) + one.astype(jnp.float32) + two.astype(jnp.float32)

time: 177 us -> 175 us (0.989)
  blocking collectives: 119 us -> 114 us
  waiting for transfers between devices: 19.1 us -> 21.5 us
    all_to_all x1, blocking collectives: 19 us -> 13.8 us  [from_everyone(): return lax.all_to_all(copies, axis, split_axis=0, concat_axis=0, tiled=True)]
    ppermute x7, waiting for transfers between devices: 19.1 us -> 21.5 us  [send(): return lax.ppermute(value, 'tp', [(t, (t + step) % tp) for t in range(tp)])]
  transfers between devices with their start and end apart: 7 -> 7, of which waited for: 5 -> 4; matrix products, arithmetic and copies ran while one was open for 1% -> 0% of each run, Pallas kernels for 2% -> 0%
where the time goes in v4:
time: 175 us
  blocking collectives  114 us (65%)
  starting transfers between devices  23.9 us (14%)
  waiting for transfers between devices  21.5 us (12%)
  Pallas kernels  8.81 us (5%)
  other arithmetic  3.49 us (2%)
  local copies, waits for them, and re-layouts  2.85 us (2%)
    all_gather x1, blocking collectives, shards(): lax.all_gather(packed.astype(jnp.float16), 'fs', axis=0, tiled=False)  100 us
    ppermute x7, starting transfers between devices, send(): return lax.ppermute(value, 'tp', [(t, (t + step) % tp) for t in range(tp)])  23.9 us
    ppermute x7, waiting for transfers between devices, send(): return lax.ppermute(value, 'tp', [(t, (t + step) % tp) for t in range(tp)])  21.5 us
    all_to_all x1, blocking collectives, from_everyone(): return lax.all_to_all(copies, axis, split_axis=0, concat_axis=0, tiled=True)  13.8 us
    pallas_call x1, Pallas kernels, first(): pl.pallas_call(first_kernel, grid=(count // rows,), in_specs=[pl.BlockSpe...  5.26 us
  transfers between devices with their start and end apart: 7, of which 4 were waited for; matrix products, arithmetic and copies ran while one was open for 0% of the time, Pallas kernels for 0%

profile of v4, /device:TPU:80, one launch (start us, length us, event | category | flops | bytes accessed | tf_op | source)
XLA Modules:
  0.0 174.7 jit_solution(16199379827023490312)
XLA Ops:
  0.0 0.0 copy-start.1
  0.0 0.9 copy-done.1
  0.9 0.0 copy-start.2
  0.9 0.9 copy-done.2
  1.8 0.7 pack.1
  2.6 100.1 %all-gather.2 = f16[16640,256]{1,0:T(8,128)(2,1)S(1)} all-gather(f16[520,256]{1,0:T(8,128)(2,1)S(1)} %convert_element_type.72), channel_id=2, replica_groups=mesh['grp'=2,'fs'=32,'tp'=8] {'fs'}, dimensions={0}, use_global_device_ids=true | all-gather | bytes 8785920 | tf_op jit(solution)/shard_map/all_gather | solution.py:198
  102.7 0.2 slice_convert_fusion.2.down_ref
  102.9 0.0 copy-start
  102.9 0.0 copy-start.3
  102.9 0.8 slice_convert_fusion.up_ref
  103.8 1.0 copy-done
  104.8 0.0 copy-done.3
  104.8 5.3 %first.1 = (bf16[768,1024]{1,0:T(8,128)(2,1)S(1)}, bf16[768,256]{1,0:T(8,128)(2,1)S(1)}, bf16[768,256]{1,0:T(8,128)(2,1)S(1)}) custom-call(bf16[768,2048]{1,0:T(8,128)(2,1)S(1)} %copy-done, f32[1,2048]{1,0:T(1,128)S(1)} %bitcast.2, bf16[32,256,256]{2,1,0:T(8,128)(2,1)S(1)} %slice_convert_fusion.up_ref, ...), custom_call_target="tpu_custom_call" | custom-call | tf_op jit(solution)/shard_map/first/pallas_call | solution.py:131
  110.1 0.6 slice_convert_fusion.1.down_ref
  110.7 2.7 %rest.2 = (bf16[768,256]{1,0:T(8,128)(2,1)S(1)}, bf16[768,256]{1,0:T(8,128)(2,1)S(1)}, bf16[768,256]{1,0:T(8,128)(2,1)S(1)}, bf16[768,256]{1,0:T(8,128)(2,1)S(1)...) custom-call(bf16[768,1024]{1,0:T(8,128)(2,1)S(1)} %get-tuple-element.31.hidden_ref, ...), custom_call_target="tpu_custom_call" | custom-call | tf_op jit(solution)/shard_map/rest/pallas_call | solution.py:172
  113.4 3.6 %collective-permute-start = (bf16[768,256]{1,0:T(8,128)(2,1)S(1)}, bf16[768,256]{1,0:T(8,128)(2,1)S(1)}, u32[]{:S(2)}, u32[]{:S(2)}) collective-permute-start(bf16[768,256]{1,0:T(8,128)(2,1)S(1)} %get-tuple-element.48), channel_id=1, source_target_pairs={{0,1},{1,2},{2,3},{3,4},{4,5},{5,6},{6,7},{7,0},{8,9},{9,10},{10,1... | collective-permute-start | bytes 1179656 | tf_op jit(solution)/shard_map/ppermute | solution.py:208
  116.9 4.1 %collective-permute-start.4 = (bf16[768,256]{1,0:T(8,128)(2,1)S(1)}, bf16[768,256]{1,0:T(8,128)(2,1)S(1)}, u32[]{:S(2)}, u32[]{:S(2)}) collective-permute-start(bf16[768,256]{1,0:T(8,128)(2,1)S(1)} %get-tuple-element.52), channel_id=1, source_target_pairs={{0,7},{1,0},{2,1},{3,2},{4,3},{5,4},{6,5},{7,6},{8,15},{9,8},{10,9... | collective-permute-start | bytes 1179656 | tf_op jit(solution)/shard_map/ppermute | solution.py:208
  121.1 0.2 rest.3
  121.3 0.0 copy-start.4
  121.3 4.8 %collective-permute-done = bf16[768,256]{1,0:T(8,128)(2,1)S(1)} collective-permute-done((bf16[768,256]{1,0:T(8,128)(2,1)S(1)}, bf16[768,256]{1,0:T(8,128)(2,1)S(1)}, u32[]{:S(2)}, u32[]{:S(2)}) %collective-permute-start) | collective-permute-done | bytes 393248 | tf_op jit(solution)/shard_map/ppermute | solution.py:208
  126.1 0.1 add_convert_fusion.4
  126.2 2.0 %collective-permute-start.1 = (bf16[768,256]{1,0:T(8,128)(2,1)S(1)}, bf16[768,256]{1,0:T(8,128)(2,1)S(1)}, u32[]{:S(2)}, u32[]{:S(2)}) collective-permute-start(bf16[768,256]{1,0:T(8,128)(2,1)S(1)} %add_convert_fusion.4), channel_id=1, source_target_pairs={{0,1},{1,2},{2,3},{3,4},{4,5},{5,6},{6,7},{7,0},{8,9},{9,10},{10,1... | collective-permute-start | bytes 1179656 | tf_op jit(solution)/shard_map/ppermute | solution.py:208
  128.2 0.0 collective-permute-done.4
  128.2 0.1 add_convert_fusion.1
  128.3 5.2 %collective-permute-start.5 = (bf16[768,256]{1,0:T(8,128)(2,1)S(1)}, bf16[768,256]{1,0:T(8,128)(2,1)S(1)}, u32[]{:S(2)}, u32[]{:S(2)}) collective-permute-start(bf16[768,256]{1,0:T(8,128)(2,1)S(1)} %add_convert_fusion.1), channel_id=1, source_target_pairs={{0,7},{1,0},{2,1},{3,2},{4,3},{5,4},{6,5},{7,6},{8,15},{9,8},{10,9... | collective-permute-start | bytes 1179656 | tf_op jit(solution)/shard_map/ppermute | solution.py:208
  133.5 4.0 %collective-permute-done.1 = bf16[768,256]{1,0:T(8,128)(2,1)S(1)} collective-permute-done((bf16[768,256]{1,0:T(8,128)(2,1)S(1)}, bf16[768,256]{1,0:T(8,128)(2,1)S(1)}, u32[]{:S(2)}, u32[]{:S(2)}) %collective-permute-start.1) | collective-permute-done | bytes 393248 | tf_op jit(solution)/shard_map/ppermute | solution.py:208
  137.5 0.1 add_convert_fusion.3
  137.7 2.0 %collective-permute-start.2 = (bf16[768,256]{1,0:T(8,128)(2,1)S(1)}, bf16[768,256]{1,0:T(8,128)(2,1)S(1)}, u32[]{:S(2)}, u32[]{:S(2)}) collective-permute-start(bf16[768,256]{1,0:T(8,128)(2,1)S(1)} %add_convert_fusion.3), channel_id=1, source_target_pairs={{0,1},{1,2},{2,3},{3,4},{4,5},{5,6},{6,7},{7,0},{8,9},{9,10},{10,1... | collective-permute-start | bytes 1179656 | tf_op jit(solution)/shard_map/ppermute | solution.py:208
  139.6 0.0 collective-permute-done.5
  139.6 0.1 add_convert_fusion
  139.7 5.2 %collective-permute-start.6 = (bf16[768,256]{1,0:T(8,128)(2,1)S(1)}, bf16[768,256]{1,0:T(8,128)(2,1)S(1)}, u32[]{:S(2)}, u32[]{:S(2)}) collective-permute-start(bf16[768,256]{1,0:T(8,128)(2,1)S(1)} %add_convert_fusion), channel_id=1, source_target_pairs={{0,7},{1,0},{2,1},{3,2},{4,3},{5,4},{6,5},{7,6},{8,15},{9,8},{10,9... | collective-permute-start | bytes 1179656 | tf_op jit(solution)/shard_map/ppermute | solution.py:208
  144.9 3.7 %collective-permute-done.2 = bf16[768,256]{1,0:T(8,128)(2,1)S(1)} collective-permute-done((bf16[768,256]{1,0:T(8,128)(2,1)S(1)}, bf16[768,256]{1,0:T(8,128)(2,1)S(1)}, u32[]{:S(2)}, u32[]{:S(2)}) %collective-permute-start.2) | collective-permute-done | bytes 393248 | tf_op jit(solution)/shard_map/ppermute | solution.py:208
  148.6 0.1 add_convert_fusion.2
  148.7 2.0 %collective-permute-start.3 = (bf16[768,256]{1,0:T(8,128)(2,1)S(1)}, bf16[768,256]{1,0:T(8,128)(2,1)S(1)}, u32[]{:S(2)}, u32[]{:S(2)}) collective-permute-start(bf16[768,256]{1,0:T(8,128)(2,1)S(1)} %add_convert_fusion.2), channel_id=1, source_target_pairs={{0,1},{1,2},{2,3},{3,4},{4,5},{5,6},{6,7},{7,0},{8,9},{9,10},{10,1... | collective-permute-start | bytes 1179656 | tf_op jit(solution)/shard_map/ppermute | solution.py:208
  150.6 0.0 collective-permute-done.6
  150.6 8.9 %collective-permute-done.3 = bf16[768,256]{1,0:T(8,128)(2,1)S(1)} collective-permute-done((bf16[768,256]{1,0:T(8,128)(2,1)S(1)}, bf16[768,256]{1,0:T(8,128)(2,1)S(1)}, u32[]{:S(2)}, u32[]{:S(2)}) %collective-permute-start.3) | collective-permute-done | bytes 393248 | tf_op jit(solution)/shard_map/ppermute | solution.py:208
  159.6 0.2 multiply_reduce_fusion
  159.9 13.8 %all_to_all.6 = f32[8,1,768]{2,1,0:T(1,128)S(1)} all-to-all(f32[8,1,768]{2,1,0:T(1,128)S(1)} %broadcast_in_dim.2), channel_id=1, replica_groups=mesh['grp'=2,'fs'=32,'tp'=8] {'tp'}, dimensions={0} | all-to-all | bytes 49152 | tf_op jit(solution)/shard_map/all_to_all | solution.py:17
  173.7 0.0 copy-done.4
  173.7 0.9 multiply_convert_fusion
  (5 shorter events, 0.1 us)
Async XLA Ops:
  0.0 0.9 copy-start.1
  0.9 0.9 copy-start.2
  102.9 1.9 %copy-start = (bf16[768,2048]{1,0:T(8,128)(2,1)S(1)}, bf16[768,2048]{1,0:T(8,128)(2,1)}, u32[]{:S(2)}) copy-start(bf16[768,2048]{1,0:T(8,128)(2,1)} %x_ref.1) | copy-start | bytes 9437188
  102.9 1.9 %copy-start.3 = (f32[2048]{0:T(1024)S(1)}, f32[2048]{0:T(1024)}, u32[]{:S(2)}) copy-start(f32[2048]{0:T(1024)} %param.6) | copy-start | bytes 24580
  113.4 12.8 %collective-permute-start = (bf16[768,256]{1,0:T(8,128)(2,1)S(1)}, bf16[768,256]{1,0:T(8,128)(2,1)S(1)}, u32[]{:S(2)}, u32[]{:S(2)}) collective-permute-start(bf16[768,256]{1,0:T(8,128)(2,1)S(1)} %get-tuple-element.48), channel_id=1, source_target_pairs={{0,1},{1,2},{2,3},{3,4},{4,5},{5,6},{6,7},{7,0},{8,9},{9,10},{10,1... | collective-permute-start | bytes 1179656 | tf_op jit(solution)/shard_map/ppermute | solution.py:208
  116.9 11.3 %collective-permute-start.4 = (bf16[768,256]{1,0:T(8,128)(2,1)S(1)}, bf16[768,256]{1,0:T(8,128)(2,1)S(1)}, u32[]{:S(2)}, u32[]{:S(2)}) collective-permute-start(bf16[768,256]{1,0:T(8,128)(2,1)S(1)} %get-tuple-element.52), channel_id=1, source_target_pairs={{0,7},{1,0},{2,1},{3,2},{4,3},{5,4},{6,5},{7,6},{8,15},{9,8},{10,9... | collective-permute-start | bytes 1179656 | tf_op jit(solution)/shard_map/ppermute | solution.py:208
  121.3 52.4 %copy-start.4 = (f32[256]{0:T(256)S(1)}, f32[256]{0:T(256)}, u32[]{:S(2)}) copy-start(f32[256]{0:T(256)} %param.9) | copy-start | bytes 3076
  126.2 11.3 %collective-permute-start.1 = (bf16[768,256]{1,0:T(8,128)(2,1)S(1)}, bf16[768,256]{1,0:T(8,128)(2,1)S(1)}, u32[]{:S(2)}, u32[]{:S(2)}) collective-permute-start(bf16[768,256]{1,0:T(8,128)(2,1)S(1)} %add_convert_fusion.4), channel_id=1, source_target_pairs={{0,1},{1,2},{2,3},{3,4},{4,5},{5,6},{6,7},{7,0},{8,9},{9,10},{10,1... | collective-permute-start | bytes 1179656 | tf_op jit(solution)/shard_map/ppermute | solution.py:208
  128.3 11.3 %collective-permute-start.5 = (bf16[768,256]{1,0:T(8,128)(2,1)S(1)}, bf16[768,256]{1,0:T(8,128)(2,1)S(1)}, u32[]{:S(2)}, u32[]{:S(2)}) collective-permute-start(bf16[768,256]{1,0:T(8,128)(2,1)S(1)} %add_convert_fusion.1), channel_id=1, source_target_pairs={{0,7},{1,0},{2,1},{3,2},{4,3},{5,4},{6,5},{7,6},{8,15},{9,8},{10,9... | collective-permute-start | bytes 1179656 | tf_op jit(solution)/shard_map/ppermute | solution.py:208
  137.7 10.9 %collective-permute-start.2 = (bf16[768,256]{1,0:T(8,128)(2,1)S(1)}, bf16[768,256]{1,0:T(8,128)(2,1)S(1)}, u32[]{:S(2)}, u32[]{:S(2)}) collective-permute-start(bf16[768,256]{1,0:T(8,128)(2,1)S(1)} %add_convert_fusion.3), channel_id=1, source_target_pairs={{0,1},{1,2},{2,3},{3,4},{4,5},{5,6},{6,7},{7,0},{8,9},{9,10},{10,1... | collective-permute-start | bytes 1179656 | tf_op jit(solution)/shard_map/ppermute | solution.py:208
  139.7 10.9 %collective-permute-start.6 = (bf16[768,256]{1,0:T(8,128)(2,1)S(1)}, bf16[768,256]{1,0:T(8,128)(2,1)S(1)}, u32[]{:S(2)}, u32[]{:S(2)}) collective-permute-start(bf16[768,256]{1,0:T(8,128)(2,1)S(1)} %add_convert_fusion), channel_id=1, source_target_pairs={{0,7},{1,0},{2,1},{3,2},{4,3},{5,4},{6,5},{7,6},{8,15},{9,8},{10,9... | collective-permute-start | bytes 1179656 | tf_op jit(solution)/shard_map/ppermute | solution.py:208
  148.7 10.9 %collective-permute-start.3 = (bf16[768,256]{1,0:T(8,128)(2,1)S(1)}, bf16[768,256]{1,0:T(8,128)(2,1)S(1)}, u32[]{:S(2)}, u32[]{:S(2)}) collective-permute-start(bf16[768,256]{1,0:T(8,128)(2,1)S(1)} %add_convert_fusion.2), channel_id=1, source_target_pairs={{0,1},{1,2},{2,3},{3,4},{4,5},{5,6},{6,7},{7,0},{8,9},{9,10},{10,1... | collective-permute-start | bytes 1179656 | tf_op jit(solution)/shard_map/ppermute | solution.py:208

commit v5 on v4

--- a/solution.py
+++ b/solution.py
@@ -190,9 +190,9 @@
     own = post_gain.shape[0]
     up_rows = up_weight.size // own
     down_rows = down_weight.shape[0]
-    offsets = [tp // 2, tp // 2 + 1, tp // 2 - 1]
+    offsets = [tp // 2, tp // 2 - 1, tp // 2 + 1]
     for distance in range(tp // 2 - 2, 0, -1):
-        offsets += [distance, tp - distance]
+        offsets += [tp - distance, distance]
     offsets.append(0)
     packed = pack(up_weight, down_weight, own, offsets)
     everything = lax.all_gather(packed.astype(jnp.float16), "fs", axis=0, tiled=False)
@@ -211,13 +211,13 @@
     rest_down = down(held, 2, tp)
     parts = rest(hidden, rest_down, [], 0)
     one, two, *parts = lax.optimization_barrier((one, two, *parts))
-    one = send(one, 1)
-    two = send(two, -1)
+    one = send(one, -1)
+    two = send(two, 1)
     part_one, *parts, own_part = rest(hidden, rest_down, parts, 1)
-    one = send(add(one, part_one), 1)
+    one = send(add(one, part_one), -1)
     for step in range(tp // 2 - 2):
-        two = send(add(two, parts[2 * step + 1]), -1)
-        one = send(add(one, parts[2 * step]), 1)
+        two = send(add(two, parts[2 * step + 1]), 1)
+        one = send(add(one, parts[2 * step]), -1)
     mixed = own_part.astype(jnp.float32) + one.astype(jnp.float32) + two.astype(jnp.float32)
     squares = of_everyone(jnp.sum(mixed * mixed, axis=1), "tp")
     factor = lax.rsqrt(squares / (tp * own) + eps)

time: 175 us -> 173 us (0.989)
  waiting for transfers between devices: 21.5 us -> 16 us
  starting transfers between devices: 23.9 us -> 28.5 us
    ppermute x7, waiting for transfers between devices: 21.5 us -> 16 us  [send(): return lax.ppermute(value, 'tp', [(t, (t + step) % tp) for t in range(tp)])]
    ppermute x7, starting transfers between devices: 23.9 us -> 28.5 us  [send(): return lax.ppermute(value, 'tp', [(t, (t + step) % tp) for t in range(tp)])]
where the time goes in v5:
time: 173 us
  blocking collectives  113 us (65%)
  starting transfers between devices  28.5 us (16%)
  waiting for transfers between devices  16 us (9%)
  Pallas kernels  8.81 us (5%)
  other arithmetic  3.49 us (2%)
  local copies, waits for them, and re-layouts  2.85 us (2%)
    all_gather x1, blocking collectives, shards(): lax.all_gather(packed.astype(jnp.float16), 'fs', axis=0, tiled=False)  100 us
    ppermute x7, starting transfers between devices, send(): return lax.ppermute(value, 'tp', [(t, (t + step) % tp) for t in range(tp)])  28.5 us
    ppermute x7, waiting for transfers between devices, send(): return lax.ppermute(value, 'tp', [(t, (t + step) % tp) for t in range(tp)])  16 us
    all_to_all x1, blocking collectives, from_everyone(): return lax.all_to_all(copies, axis, split_axis=0, concat_axis=0, tiled=True)  12.6 us
    pallas_call x1, Pallas kernels, first(): pl.pallas_call(first_kernel, grid=(count // rows,), in_specs=[pl.BlockSpe...  5.26 us
  transfers between devices with their start and end apart: 7, of which 4 were waited for; matrix products, arithmetic and copies ran while one was open for 0% of the time, Pallas kernels for 0%

profile of v5, /device:TPU:80, one launch (start us, length us, event | category | flops | bytes accessed | tf_op | source)
XLA Modules:
  0.0 172.5 jit_solution(1818987179909221250)
XLA Ops:
  0.0 0.0 copy-start.1
  0.0 0.9 copy-done.1
  0.9 0.0 copy-start.2
  0.9 0.9 copy-done.2
  1.8 0.7 pack.1
  2.6 100.1 %all-gather.2 = f16[16640,256]{1,0:T(8,128)(2,1)S(1)} all-gather(f16[520,256]{1,0:T(8,128)(2,1)S(1)} %convert_element_type.72), channel_id=2, replica_groups=mesh['grp'=2,'fs'=32,'tp'=8] {'fs'}, dimensions={0}, use_global_device_ids=true | all-gather | bytes 8785920 | tf_op jit(solution)/shard_map/all_gather | solution.py:198
  102.7 0.2 slice_convert_fusion.2.down_ref
  102.9 0.0 copy-start
  102.9 0.0 copy-start.3
  102.9 0.8 slice_convert_fusion.up_ref
  103.8 1.0 copy-done
  104.8 0.0 copy-done.3
  104.8 5.3 %first.1 = (bf16[768,1024]{1,0:T(8,128)(2,1)S(1)}, bf16[768,256]{1,0:T(8,128)(2,1)S(1)}, bf16[768,256]{1,0:T(8,128)(2,1)S(1)}) custom-call(bf16[768,2048]{1,0:T(8,128)(2,1)S(1)} %copy-done, f32[1,2048]{1,0:T(1,128)S(1)} %bitcast.2, bf16[32,256,256]{2,1,0:T(8,128)(2,1)S(1)} %slice_convert_fusion.up_ref, ...), custom_call_target="tpu_custom_call" | custom-call | tf_op jit(solution)/shard_map/first/pallas_call | solution.py:131
  110.1 0.6 slice_convert_fusion.1.down_ref
  110.7 2.7 %rest.2 = (bf16[768,256]{1,0:T(8,128)(2,1)S(1)}, bf16[768,256]{1,0:T(8,128)(2,1)S(1)}, bf16[768,256]{1,0:T(8,128)(2,1)S(1)}, bf16[768,256]{1,0:T(8,128)(2,1)S(1)...) custom-call(bf16[768,1024]{1,0:T(8,128)(2,1)S(1)} %get-tuple-element.31.hidden_ref, ...), custom_call_target="tpu_custom_call" | custom-call | tf_op jit(solution)/shard_map/rest/pallas_call | solution.py:172
  113.4 5.8 %collective-permute-start = (bf16[768,256]{1,0:T(8,128)(2,1)S(1)}, bf16[768,256]{1,0:T(8,128)(2,1)S(1)}, u32[]{:S(2)}, u32[]{:S(2)}) collective-permute-start(bf16[768,256]{1,0:T(8,128)(2,1)S(1)} %get-tuple-element.48), channel_id=1, source_target_pairs={{0,7},{1,0},{2,1},{3,2},{4,3},{5,4},{6,5},{7,6},{8,15},{9,8},{10,9... | collective-permute-start | bytes 1179656 | tf_op jit(solution)/shard_map/ppermute | solution.py:208
  119.1 2.0 %collective-permute-start.4 = (bf16[768,256]{1,0:T(8,128)(2,1)S(1)}, bf16[768,256]{1,0:T(8,128)(2,1)S(1)}, u32[]{:S(2)}, u32[]{:S(2)}) collective-permute-start(bf16[768,256]{1,0:T(8,128)(2,1)S(1)} %get-tuple-element.52), channel_id=1, source_target_pairs={{0,1},{1,2},{2,3},{3,4},{4,5},{5,6},{6,7},{7,0},{8,9},{9,10},{10,1... | collective-permute-start | bytes 1179656 | tf_op jit(solution)/shard_map/ppermute | solution.py:208
  121.1 0.2 rest.3
  121.3 0.0 copy-start.4
  121.3 4.1 %collective-permute-done = bf16[768,256]{1,0:T(8,128)(2,1)S(1)} collective-permute-done((bf16[768,256]{1,0:T(8,128)(2,1)S(1)}, bf16[768,256]{1,0:T(8,128)(2,1)S(1)}, u32[]{:S(2)}, u32[]{:S(2)}) %collective-permute-start) | collective-permute-done | bytes 393248 | tf_op jit(solution)/shard_map/ppermute | solution.py:208
  125.4 0.1 add_convert_fusion.4
  125.5 5.6 %collective-permute-start.1 = (bf16[768,256]{1,0:T(8,128)(2,1)S(1)}, bf16[768,256]{1,0:T(8,128)(2,1)S(1)}, u32[]{:S(2)}, u32[]{:S(2)}) collective-permute-start(bf16[768,256]{1,0:T(8,128)(2,1)S(1)} %add_convert_fusion.4), channel_id=1, source_target_pairs={{0,7},{1,0},{2,1},{3,2},{4,3},{5,4},{6,5},{7,6},{8,15},{9,8},{10,9... | collective-permute-start | bytes 1179656 | tf_op jit(solution)/shard_map/ppermute | solution.py:208
  131.1 0.0 collective-permute-done.4
  131.1 0.1 add_convert_fusion.1
  131.3 2.0 %collective-permute-start.5 = (bf16[768,256]{1,0:T(8,128)(2,1)S(1)}, bf16[768,256]{1,0:T(8,128)(2,1)S(1)}, u32[]{:S(2)}, u32[]{:S(2)}) collective-permute-start(bf16[768,256]{1,0:T(8,128)(2,1)S(1)} %add_convert_fusion.1), channel_id=1, source_target_pairs={{0,1},{1,2},{2,3},{3,4},{4,5},{5,6},{6,7},{7,0},{8,9},{9,10},{10,1... | collective-permute-start | bytes 1179656 | tf_op jit(solution)/shard_map/ppermute | solution.py:208
  133.2 3.3 %collective-permute-done.1 = bf16[768,256]{1,0:T(8,128)(2,1)S(1)} collective-permute-done((bf16[768,256]{1,0:T(8,128)(2,1)S(1)}, bf16[768,256]{1,0:T(8,128)(2,1)S(1)}, u32[]{:S(2)}, u32[]{:S(2)}) %collective-permute-start.1) | collective-permute-done | bytes 393248 | tf_op jit(solution)/shard_map/ppermute | solution.py:208
  136.5 0.1 add_convert_fusion.3
  136.6 5.6 %collective-permute-start.2 = (bf16[768,256]{1,0:T(8,128)(2,1)S(1)}, bf16[768,256]{1,0:T(8,128)(2,1)S(1)}, u32[]{:S(2)}, u32[]{:S(2)}) collective-permute-start(bf16[768,256]{1,0:T(8,128)(2,1)S(1)} %add_convert_fusion.3), channel_id=1, source_target_pairs={{0,7},{1,0},{2,1},{3,2},{4,3},{5,4},{6,5},{7,6},{8,15},{9,8},{10,9... | collective-permute-start | bytes 1179656 | tf_op jit(solution)/shard_map/ppermute | solution.py:208
  142.3 0.0 collective-permute-done.5
  142.3 0.1 add_convert_fusion
  142.4 2.0 %collective-permute-start.6 = (bf16[768,256]{1,0:T(8,128)(2,1)S(1)}, bf16[768,256]{1,0:T(8,128)(2,1)S(1)}, u32[]{:S(2)}, u32[]{:S(2)}) collective-permute-start(bf16[768,256]{1,0:T(8,128)(2,1)S(1)} %add_convert_fusion), channel_id=1, source_target_pairs={{0,1},{1,2},{2,3},{3,4},{4,5},{5,6},{6,7},{7,0},{8,9},{9,10},{10,1... | collective-permute-start | bytes 1179656 | tf_op jit(solution)/shard_map/ppermute | solution.py:208
  144.3 3.2 %collective-permute-done.2 = bf16[768,256]{1,0:T(8,128)(2,1)S(1)} collective-permute-done((bf16[768,256]{1,0:T(8,128)(2,1)S(1)}, bf16[768,256]{1,0:T(8,128)(2,1)S(1)}, u32[]{:S(2)}, u32[]{:S(2)}) %collective-permute-start.2) | collective-permute-done | bytes 393248 | tf_op jit(solution)/shard_map/ppermute | solution.py:208
  147.5 0.1 add_convert_fusion.2
  147.7 5.6 %collective-permute-start.3 = (bf16[768,256]{1,0:T(8,128)(2,1)S(1)}, bf16[768,256]{1,0:T(8,128)(2,1)S(1)}, u32[]{:S(2)}, u32[]{:S(2)}) collective-permute-start(bf16[768,256]{1,0:T(8,128)(2,1)S(1)} %add_convert_fusion.2), channel_id=1, source_target_pairs={{0,7},{1,0},{2,1},{3,2},{4,3},{5,4},{6,5},{7,6},{8,15},{9,8},{10,9... | collective-permute-start | bytes 1179656 | tf_op jit(solution)/shard_map/ppermute | solution.py:208
  153.3 0.0 collective-permute-done.6
  153.3 5.4 %collective-permute-done.3 = bf16[768,256]{1,0:T(8,128)(2,1)S(1)} collective-permute-done((bf16[768,256]{1,0:T(8,128)(2,1)S(1)}, bf16[768,256]{1,0:T(8,128)(2,1)S(1)}, u32[]{:S(2)}, u32[]{:S(2)}) %collective-permute-start.3) | collective-permute-done | bytes 393248 | tf_op jit(solution)/shard_map/ppermute | solution.py:208
  158.7 0.2 multiply_reduce_fusion
  158.9 12.6 %all_to_all.6 = f32[8,1,768]{2,1,0:T(1,128)S(1)} all-to-all(f32[8,1,768]{2,1,0:T(1,128)S(1)} %broadcast_in_dim.2), channel_id=1, replica_groups=mesh['grp'=2,'fs'=32,'tp'=8] {'tp'}, dimensions={0} | all-to-all | bytes 49152 | tf_op jit(solution)/shard_map/all_to_all | solution.py:17
  171.6 0.0 copy-done.4
  171.6 0.9 multiply_convert_fusion
  (5 shorter events, 0.1 us)
Async XLA Ops:
  0.0 0.9 copy-start.1
  0.9 0.9 copy-start.2
  102.9 1.9 %copy-start = (bf16[768,2048]{1,0:T(8,128)(2,1)S(1)}, bf16[768,2048]{1,0:T(8,128)(2,1)}, u32[]{:S(2)}) copy-start(bf16[768,2048]{1,0:T(8,128)(2,1)} %x_ref.1) | copy-start | bytes 9437188
  102.9 1.9 %copy-start.3 = (f32[2048]{0:T(1024)S(1)}, f32[2048]{0:T(1024)}, u32[]{:S(2)}) copy-start(f32[2048]{0:T(1024)} %param.6) | copy-start | bytes 24580
  113.4 12.0 %collective-permute-start = (bf16[768,256]{1,0:T(8,128)(2,1)S(1)}, bf16[768,256]{1,0:T(8,128)(2,1)S(1)}, u32[]{:S(2)}, u32[]{:S(2)}) collective-permute-start(bf16[768,256]{1,0:T(8,128)(2,1)S(1)} %get-tuple-element.48), channel_id=1, source_target_pairs={{0,7},{1,0},{2,1},{3,2},{4,3},{5,4},{6,5},{7,6},{8,15},{9,8},{10,9... | collective-permute-start | bytes 1179656 | tf_op jit(solution)/shard_map/ppermute | solution.py:208
  119.1 12.0 %collective-permute-start.4 = (bf16[768,256]{1,0:T(8,128)(2,1)S(1)}, bf16[768,256]{1,0:T(8,128)(2,1)S(1)}, u32[]{:S(2)}, u32[]{:S(2)}) collective-permute-start(bf16[768,256]{1,0:T(8,128)(2,1)S(1)} %get-tuple-element.52), channel_id=1, source_target_pairs={{0,1},{1,2},{2,3},{3,4},{4,5},{5,6},{6,7},{7,0},{8,9},{9,10},{10,1... | collective-permute-start | bytes 1179656 | tf_op jit(solution)/shard_map/ppermute | solution.py:208
  121.3 50.3 %copy-start.4 = (f32[256]{0:T(256)S(1)}, f32[256]{0:T(256)}, u32[]{:S(2)}) copy-start(f32[256]{0:T(256)} %param.9) | copy-start | bytes 3076
  125.5 11.0 %collective-permute-start.1 = (bf16[768,256]{1,0:T(8,128)(2,1)S(1)}, bf16[768,256]{1,0:T(8,128)(2,1)S(1)}, u32[]{:S(2)}, u32[]{:S(2)}) collective-permute-start(bf16[768,256]{1,0:T(8,128)(2,1)S(1)} %add_convert_fusion.4), channel_id=1, source_target_pairs={{0,7},{1,0},{2,1},{3,2},{4,3},{5,4},{6,5},{7,6},{8,15},{9,8},{10,9... | collective-permute-start | bytes 1179656 | tf_op jit(solution)/shard_map/ppermute | solution.py:208
  131.3 11.0 %collective-permute-start.5 = (bf16[768,256]{1,0:T(8,128)(2,1)S(1)}, bf16[768,256]{1,0:T(8,128)(2,1)S(1)}, u32[]{:S(2)}, u32[]{:S(2)}) collective-permute-start(bf16[768,256]{1,0:T(8,128)(2,1)S(1)} %add_convert_fusion.1), channel_id=1, source_target_pairs={{0,1},{1,2},{2,3},{3,4},{4,5},{5,6},{6,7},{7,0},{8,9},{9,10},{10,1... | collective-permute-start | bytes 1179656 | tf_op jit(solution)/shard_map/ppermute | solution.py:208
  136.6 10.9 %collective-permute-start.2 = (bf16[768,256]{1,0:T(8,128)(2,1)S(1)}, bf16[768,256]{1,0:T(8,128)(2,1)S(1)}, u32[]{:S(2)}, u32[]{:S(2)}) collective-permute-start(bf16[768,256]{1,0:T(8,128)(2,1)S(1)} %add_convert_fusion.3), channel_id=1, source_target_pairs={{0,7},{1,0},{2,1},{3,2},{4,3},{5,4},{6,5},{7,6},{8,15},{9,8},{10,9... | collective-permute-start | bytes 1179656 | tf_op jit(solution)/shard_map/ppermute | solution.py:208
  142.4 10.9 %collective-permute-start.6 = (bf16[768,256]{1,0:T(8,128)(2,1)S(1)}, bf16[768,256]{1,0:T(8,128)(2,1)S(1)}, u32[]{:S(2)}, u32[]{:S(2)}) collective-permute-start(bf16[768,256]{1,0:T(8,128)(2,1)S(1)} %add_convert_fusion), channel_id=1, source_target_pairs={{0,1},{1,2},{2,3},{3,4},{4,5},{5,6},{6,7},{7,0},{8,9},{9,10},{10,1... | collective-permute-start | bytes 1179656 | tf_op jit(solution)/shard_map/ppermute | solution.py:208
  147.7 11.0 %collective-permute-start.3 = (bf16[768,256]{1,0:T(8,128)(2,1)S(1)}, bf16[768,256]{1,0:T(8,128)(2,1)S(1)}, u32[]{:S(2)}, u32[]{:S(2)}) collective-permute-start(bf16[768,256]{1,0:T(8,128)(2,1)S(1)} %add_convert_fusion.2), channel_id=1, source_target_pairs={{0,7},{1,0},{2,1},{3,2},{4,3},{5,4},{6,5},{7,6},{8,15},{9,8},{10,9... | collective-permute-start | bytes 1179656 | tf_op jit(solution)/shard_map/ppermute | solution.py:208
